TPU v7x, 32 devices: a whole 2x2x4 slice. The times are simulated.
32 devices in a mesh: ep: 8 (over z, core), tp: 4 (over y, x).
Axes of the slice: x: 2, y: 2, z: 4, core: 2. Of those that a mesh axis runs over, the one named last changes fastest.
Arguments:
- query_pairs: bfloat16 [3072, 2048], P('ep', 'tp'), may hold values from -64 to 64
- key_pairs: bfloat16 [3072, 2048], P('ep', 'tp'), may hold values from -64 to 64
- value_rows: bfloat16 [3072, 2048], P('ep', 'tp'), may hold values from -6 to 6
- head_lambda: float32 [16], P('tp'), may hold values from 0.3 to 0.8
- head_gain: float32 [128], replicated, may hold values from 0.1 to 1.9
- out_weight: bfloat16 [2048, 2048], P('tp'), may hold values from -0.1875 to 0.1875
- moe_input: bfloat16 [1280, 2048], P('ep'), may hold values from -6 to 6
- ffn_gain: float32 [2048], replicated, may hold values from 0.1 to 1.9
- routes: int32 [1280, 2], P('ep'), may hold values from 0 to 7, all different within a row; in each aligned block of 160 rows (0 to 159, 160 to 319, ...) at most 50 rows name the same one
- route_weight: float32 [1280, 2], P('ep'), may hold values from 0.25 to 2.5
- gate_weight: bfloat16 [8, 2048, 2048], P('ep', None, 'tp'), may hold values from -0.125 to 0.125
- up_weight: bfloat16 [8, 2048, 2048], P('ep', None, 'tp'), may hold values from -0.125 to 0.125
- down_weight: bfloat16 [8, 2048, 2048], P('ep', 'tp'), may hold values from -0.1875 to 0.1875
- shared_gate: bfloat16 [2048, 2048], P(None, 'tp'), may hold values from -0.125 to 0.125
- shared_up: bfloat16 [2048, 2048], P(None, 'tp'), may hold values from -0.125 to 0.125
- shared_down: bfloat16 [2048, 2048], P('tp'), may hold values from -0.1875 to 0.1875
Outputs:
- attn_out: bfloat16 [3072, 2048], P('ep', 'tp')
- moe_out: bfloat16 [1280, 2048], P('ep', 'tp')
Inputs may be any that keep to these rules, and one draw needn't show every extreme that they name: `routes`: in each aligned block of 160 rows (the rows of one device along ep) no expert is named more than 50 times, a bound that some block reaches; a row names 2 different experts.
All inputs are finite; a program needn't handle non-finite values.
Results may differ from a plain program's by a relative error of at most 0.017.
The roundings to bfloat16 on the way count: a program that leaves them out, or rounds other values in their place, can miss the bound.
Values may be sent and summed in bfloat16 or wider, within the bound.
A program may use at most 64 MiB of HBM per device.

v0:
```python
import jax
import jax.numpy as jnp
from jax import lax
from jax.sharding import PartitionSpec as P

TOP_K = 2
KEY_BLOCK = 128


theta_base = 500000.0
norm_eps = 1e-06
masked_low = -1e30


def rotate(inputs, positions):
    half_size = inputs.shape[-1] // 2
    frequency = theta_base ** (-(jnp.arange(half_size, dtype=jnp.float32) * 2.0) / inputs.shape[-1])
    angles = positions.astype(jnp.float32)[:, None] * frequency[None, :]
    cosine = jnp.cos(angles)[:, None, None, :]
    sine_part = jnp.sin(angles)[:, None, None, :]
    front_half = inputs[..., :half_size]
    back_half = inputs[..., half_size:]
    return jnp.concatenate(
        [front_half * cosine - back_half * sine_part, back_half * cosine + front_half * sine_part],
        axis=-1,
    )


def local(
    query_pairs,
    key_pairs,
    value_rows,
    head_lambda,
    head_gain,
    out_weight,
    moe_input,
    ffn_gain,
    routes,
    route_weight,
    gate_weight,
    up_weight,
    down_weight,
    shared_gate,
    shared_up,
    shared_down,
):
    local_rows = query_pairs.shape[0]
    local_heads = head_lambda.shape[0]
    head_size = query_pairs.shape[1] // (2 * local_heads)
    value_size = value_rows.shape[1] // local_heads
    positions = lax.axis_index("ep") * local_rows + jnp.arange(local_rows, dtype=jnp.int32)
    rot_queries = rotate(
        query_pairs.astype(jnp.float32).reshape(local_rows, local_heads, 2, head_size), positions
    ).astype(jnp.bfloat16)
    rot_keys = rotate(
        key_pairs.astype(jnp.float32).reshape(local_rows, local_heads, 2, head_size), positions
    ).astype(jnp.bfloat16)
    rot_keys = rot_keys.reshape(local_rows, local_heads * 2 * head_size)
    zero_init = (
        jnp.full((local_heads, 2, local_rows), masked_low, jnp.float32),
        jnp.zeros((local_heads, 2, local_rows), jnp.float32),
        jnp.zeros((local_heads, 2, local_rows, value_size), jnp.float32),
    )
    piece_keys = lax.all_gather(rot_keys, "ep", axis=0, tiled=True)
    piece_values = lax.all_gather(value_rows, "ep", axis=0, tiled=True)
    block_count = piece_keys.shape[0] // KEY_BLOCK
    group_size = 4
    group_count = block_count // group_size
    grouped_keys = piece_keys.reshape(group_count, group_size, KEY_BLOCK, local_heads, 2, head_size)
    grouped_values = piece_values.reshape(
        group_count, group_size, KEY_BLOCK, local_heads, value_size
    )

    def one_group(current, inputs):
        block_keys, block_values, group_index = inputs
        key_positions = group_index * group_size * KEY_BLOCK + jnp.arange(
            group_size * KEY_BLOCK, dtype=jnp.int32
        ).reshape(group_size, KEY_BLOCK)
        scores = jnp.einsum(
            "qhmd,gkhmd->hmqgk", rot_queries, block_keys, preferred_element_type=jnp.float32
        ) * head_size ** (-0.5)
        allowed = key_positions[None, :, :] <= positions[:, None, None]
        scores = jnp.where(allowed, scores, masked_low)
        block_max = jnp.max(scores, axis=-1)
        weights = jnp.where(allowed, jnp.exp(scores - block_max[..., None]), 0.0)
        block_sum = jnp.sum(weights, axis=-1)
        block_out = jnp.einsum(
            "hmqgk,gkhc->hmqgc",
            weights.astype(jnp.bfloat16),
            block_values,
            preferred_element_type=jnp.float32,
        )
        run_max, run_sum, run_out = current
        new_max = jnp.maximum(run_max, jnp.max(block_max, axis=-1))
        old_scale = jnp.exp(run_max - new_max)
        new_scale = jnp.exp(block_max - new_max[..., None])
        run_sum = run_sum * old_scale + jnp.sum(new_scale * block_sum, axis=-1)
        run_out = run_out * old_scale[..., None] + jnp.sum(
            new_scale[..., None] * block_out, axis=-2
        )
        return ((new_max, run_sum, run_out), None)

    result, _ = lax.scan(
        one_group,
        zero_init,
        (grouped_keys, grouped_values, jnp.arange(group_count, dtype=jnp.int32)),
    )
    run_max, run_sum, run_out = result
    map_outputs = run_out / run_sum[..., None]
    difference = map_outputs[:, 0] - head_lambda[:, None, None] * map_outputs[:, 1]
    inverse_rms = lax.rsqrt(jnp.mean(difference * difference, axis=-1, keepdims=True) + norm_eps)
    normed_heads = (difference * inverse_rms * head_gain).astype(jnp.bfloat16)
    head_rows = normed_heads.transpose(1, 0, 2).reshape(local_rows, local_heads * value_size)
    mixer_terms = jnp.dot(head_rows, out_weight, preferred_element_type=jnp.float32)
    attn_out = lax.psum_scatter(
        mixer_terms.astype(jnp.bfloat16), "tp", scatter_dimension=1, tiled=True
    )
    row_values = moe_input.astype(jnp.float32)
    inverse_norm = lax.rsqrt(jnp.mean(row_values * row_values, axis=-1, keepdims=True) + norm_eps)
    normed = (row_values * inverse_norm * ffn_gain).astype(jnp.bfloat16)
    token_rows = normed.shape[0]
    experts = lax.axis_size("ep")
    capacity = token_rows * TOP_K * 5 // (4 * experts)
    flat_routes = routes.reshape(-1)
    onehot = (flat_routes[:, None] == jnp.arange(experts, dtype=jnp.int32)).astype(jnp.int32)
    slot_rank = jnp.sum((jnp.cumsum(onehot, axis=0) - 1) * onehot, axis=-1)
    slot_index = flat_routes * capacity + slot_rank
    token_index = jnp.arange(token_rows * TOP_K, dtype=jnp.int32) // TOP_K
    slot_rows = (
        jnp.full((experts * capacity,), token_rows, jnp.int32).at[slot_index].set(token_index)
    )
    padded = jnp.concatenate([normed, jnp.zeros((1, normed.shape[1]), jnp.bfloat16)], axis=0)
    outgoing = padded[slot_rows]
    arrived = lax.all_to_all(outgoing, "ep", split_axis=0, concat_axis=0, tiled=True)
    gate_part = jnp.dot(arrived, gate_weight[0], preferred_element_type=jnp.float32)
    up_part = jnp.dot(arrived, up_weight[0], preferred_element_type=jnp.float32)
    hidden = (jax.nn.silu(gate_part) * up_part).astype(jnp.bfloat16)
    expert_terms = jnp.dot(hidden, down_weight[0], preferred_element_type=jnp.float32)
    shared_gated = jnp.dot(normed, shared_gate, preferred_element_type=jnp.float32)
    shared_lifted = jnp.dot(normed, shared_up, preferred_element_type=jnp.float32)
    shared_hidden = (jax.nn.silu(shared_gated) * shared_lifted).astype(jnp.bfloat16)
    shared_terms = jnp.dot(shared_hidden, shared_down, preferred_element_type=jnp.float32)
    expert_sum, shared_sum = (
        lax.psum_scatter(
            expert_terms.astype(jnp.bfloat16), "tp", scatter_dimension=1, tiled=True
        ).astype(jnp.float32),
        lax.psum_scatter(
            shared_terms.astype(jnp.bfloat16), "tp", scatter_dimension=1, tiled=True
        ).astype(jnp.float32),
    )
    returned = lax.all_to_all(
        expert_sum.astype(jnp.bfloat16), "ep", split_axis=0, concat_axis=0, tiled=True
    )
    picked = returned[slot_index.reshape(token_rows, TOP_K)]
    moe_out = (
        jnp.sum(route_weight[..., None] * picked.astype(jnp.float32), axis=1) + shared_sum
    ).astype(jnp.bfloat16)
    return (attn_out, moe_out)


def solution(mesh):
    return jax.shard_map(
        local,
        mesh=mesh,
        in_specs=(
            P("ep", "tp"),
            P("ep", "tp"),
            P("ep", "tp"),
            P("tp"),
            P(),
            P("tp", None),
            P("ep", None),
            P(),
            P("ep", None),
            P("ep", None),
            P("ep", None, "tp"),
            P("ep", None, "tp"),
            P("ep", "tp", None),
            P(None, "tp"),
            P(None, "tp"),
            P("tp", None),
        ),
        out_specs=(P("ep", "tp"), P("ep", "tp")),
        check_vma=False,
    )
```

profile of v0, /device:TPU:0, one launch (start us, length us, event | category | flops | bytes accessed | tf_op | source)
XLA Modules:
  0.0 278.8 jit_solution(1547634101651810590)
XLA Ops:
  21.0 2.9 %scatter_custom_fusion = s32[400]{0:T(512)S(1)} fusion(s32[320]{0:T(512)S(1)} %fusion.51, s32[320]{0:T(512)S(1)} %add_select_fusion, s32[]{:T(128)} %constant.118.clone.1), kind=kCustom, calls=%fused_computation.100 | custom fusion | bytes 1604 | tf_op jit(solution)/shard_map/scatter | solution.py:130
  23.9 3.1 %gather_fusion = bf16[400,2048]{1,0:T(8,128)(2,1)} fusion(bf16[161,2048]{1,0:T(8,128)(2,1)S(1)} %concatenate.13, s32[1024]{0:T(1024)S(1)} %pad_clamp_fusion.1), kind=kCustom, calls=%fused_computation | custom fusion | bytes 3278400 | tf_op jit(solution)/shard_map/gather | solution.py:133
  29.7 79.5 %all_to_all.24 = bf16[8,50,2048]{2,1,0:T(8,128)(2,1)} all-to-all(bf16[8,50,2048]{2,1,0:T(8,128)(2,1)} %all_to_all.16), channel_id=1, replica_groups=mesh['ep'=8,'tp'=4] {'ep'}, dimensions={0} | all-to-all | bytes 3276800 | tf_op jit(solution)/shard_map/all_to_all | solution.py:134
  111.8 4.1 %fusion.20 = f32[400,512]{1,0:T(8,128)} fusion(bf16[400,2048]{1,0:T(8,128)(2,1)} %all_to_all.18, bf16[1,2048,512]{2,1,0:T(8,128)(2,1)} %param.28), kind=kOutput, calls=%fused_computation.38 | convolution fusion | flops 838860800 | bytes 4554752 | tf_op jit(solution)/shard_map/dot_general | solution.py:135
  115.8 5.5 %convolution_convert_fusion = bf16[400,2048]{1,0:T(8,128)(2,1)} fusion(bf16[1,512,2048]{2,1,0:T(8,128)(2,1)S(1)} %copy-done, bf16[400,2048]{1,0:T(8,128)(2,1)} %all_to_all.18, bf16[1,2048,512]{2,1,0:T(8,128)(2,1)} %param.29, f32[400,512]{1,0:T(8,128)} %fusion.20), kind=kOutput, calls=%fused_computation.32 | convolution fusion | flops 1679769600 | bytes 8290304 | tf_op jit(solution)/shard_map/dot_general | solution.py:138
  123.5 4.1 %convolution_convert_fusion.2 = bf16[160,2048]{1,0:T(8,128)(2,1)} fusion(bf16[512,2048]{1,0:T(8,128)(2,1)} %param.33, bf16[160,2048]{1,0:T(8,128)(2,1)S(1)} %fusion.24, bf16[2048,512]{1,0:T(8,128)(2,1)} %param.32, f32[160,512]{1,0:T(8,128)S(1)} %fusion.56), kind=kOutput, calls=%fused_computation.34 | convolution fusion | flops 671907840 | bytes 5832704 | tf_op jit(solution)/shard_map/dot_general | solution.py:142
  128.9 6.8 %reshape.184 = bf16[6,4,128,4,2,64]{2,1,0,5,4,3:T(4,128)(2,1)} reshape(bf16[3072,512]{0,1:T(8,128)(2,1)} %all-gather.3.cloned.1.call-done) | data formatting | bytes 6291456 | tf_op jit(solution)/shard_map/reshape | solution.py:69
  135.7 5.5 %reshape.187 = bf16[6,4,128,4,128]{4,3,2,1,0:T(4,128)(2,1)} reshape(bf16[3072,512]{1,0:T(8,128)(2,1)} %all-gather.5.cloned.1.call-done) | data formatting | bytes 6291456 | tf_op jit(solution)/shard_map/reshape | solution.py:70
  141.3 94.9 %while.17 = (s32[]{:T(128)}, f32[4,2,384]{2,1,0:T(2,128)S(1)}, f32[4,2,384]{2,1,0:T(2,128)}, f32[4,2,384,128]{2,3,1,0:T(8,128)}, s32[6]{0:T(128)S(1)}, /*index=5...) while((s32[]{:T(128)}, f32[4,2,384]{2,1,0:T(2,128)S(1)}, ...), condition=%wide.region_6.7_spmd.clone, body=%wide.region_0.6_spmd.clone.sunk | while | flops 623866752 | bytes 31223088 | solution.py:103
  145.3 3.3 %fusion.77 = (f32[4,2,384,4]{2,3,1,0:T(4,128)S(1)}, f32[4,2,384]{2,1,0:T(2,128)S(1)}, bf16[4,2,384,4,128]{2,4,3,1,0:T(8,128)(2,1)}) fusion(f32[4,2,4,128,384]{4,3,2,1,0:T(8,128)S(1)} %get-tuple-element.270, f32[4,2,384,4]{2,3,1,0:T(4,128)S(1)} %get-tuple-element.271, pred[384,4,128]{0,2,1:T(8,128)(4,1)S(1)} %broadcast_compare_fusion.2), kind=kLoop, calls=%fused_computation.9.clone.1 | loop fusion | flops 10994688 | bytes 9744384 | tf_op jit(solution)/shard_map/while/body/eval_jaxpr/reduce_sum | solution.py:86
  151.6 3.0 %fusion.80 = f32[4,2,384,128]{2,3,1,0:T(8,128)S(1)} fusion(f32[4,2,384,4]{2,1,3,0:T(2,128)} %copy.67, bf16[4,2,384,4,128]{2,4,3,1,0:T(8,128)(2,1)} %get-tuple-element.277, bf16[1,4,128,4,128]{2,4,1,3,0:T(8,128)(2,1)S(1)} %copy.68), kind=kOutput, calls=%fused_computation.5.clone.1 | convolution fusion | flops 405405696 | bytes 5292032 | tf_op jit(solution)/shard_map/while/body/eval_jaxpr/hmqgk,gkhc->hmqgc/dot_general | solution.py:87
  160.0 3.3 %fusion.77 = (f32[4,2,384,4]{2,3,1,0:T(4,128)S(1)}, f32[4,2,384]{2,1,0:T(2,128)S(1)}, bf16[4,2,384,4,128]{2,4,3,1,0:T(8,128)(2,1)}) fusion(f32[4,2,4,128,384]{4,3,2,1,0:T(8,128)S(1)} %get-tuple-element.270, f32[4,2,384,4]{2,3,1,0:T(4,128)S(1)} %get-tuple-element.271, pred[384,4,128]{0,2,1:T(8,128)(4,1)S(1)} %broadcast_compare_fusion.2), kind=kLoop, calls=%fused_computation.9.clone.1 | loop fusion | flops 10994688 | bytes 9744384 | tf_op jit(solution)/shard_map/while/body/eval_jaxpr/reduce_sum | solution.py:86
  166.3 3.0 %fusion.80 = f32[4,2,384,128]{2,3,1,0:T(8,128)S(1)} fusion(f32[4,2,384,4]{2,1,3,0:T(2,128)} %copy.67, bf16[4,2,384,4,128]{2,4,3,1,0:T(8,128)(2,1)} %get-tuple-element.277, bf16[1,4,128,4,128]{2,4,1,3,0:T(8,128)(2,1)S(1)} %copy.68), kind=kOutput, calls=%fused_computation.5.clone.1 | convolution fusion | flops 405405696 | bytes 5292032 | tf_op jit(solution)/shard_map/while/body/eval_jaxpr/hmqgk,gkhc->hmqgc/dot_general | solution.py:87
  176.0 3.3 %fusion.77 = (f32[4,2,384,4]{2,3,1,0:T(4,128)S(1)}, f32[4,2,384]{2,1,0:T(2,128)S(1)}, bf16[4,2,384,4,128]{2,4,3,1,0:T(8,128)(2,1)}) fusion(f32[4,2,4,128,384]{4,3,2,1,0:T(8,128)S(1)} %get-tuple-element.270, f32[4,2,384,4]{2,3,1,0:T(4,128)S(1)} %get-tuple-element.271, pred[384,4,128]{0,2,1:T(8,128)(4,1)S(1)} %broadcast_compare_fusion.2), kind=kLoop, calls=%fused_computation.9.clone.1 | loop fusion | flops 10994688 | bytes 9744384 | tf_op jit(solution)/shard_map/while/body/eval_jaxpr/reduce_sum | solution.py:86
  182.3 3.0 %fusion.80 = f32[4,2,384,128]{2,3,1,0:T(8,128)S(1)} fusion(f32[4,2,384,4]{2,1,3,0:T(2,128)} %copy.67, bf16[4,2,384,4,128]{2,4,3,1,0:T(8,128)(2,1)} %get-tuple-element.277, bf16[1,4,128,4,128]{2,4,1,3,0:T(8,128)(2,1)S(1)} %copy.68), kind=kOutput, calls=%fused_computation.5.clone.1 | convolution fusion | flops 405405696 | bytes 5292032 | tf_op jit(solution)/shard_map/while/body/eval_jaxpr/hmqgk,gkhc->hmqgc/dot_general | solution.py:87
  192.0 3.3 %fusion.77 = (f32[4,2,384,4]{2,3,1,0:T(4,128)S(1)}, f32[4,2,384]{2,1,0:T(2,128)S(1)}, bf16[4,2,384,4,128]{2,4,3,1,0:T(8,128)(2,1)}) fusion(f32[4,2,4,128,384]{4,3,2,1,0:T(8,128)S(1)} %get-tuple-element.270, f32[4,2,384,4]{2,3,1,0:T(4,128)S(1)} %get-tuple-element.271, pred[384,4,128]{0,2,1:T(8,128)(4,1)S(1)} %broadcast_compare_fusion.2), kind=kLoop, calls=%fused_computation.9.clone.1 | loop fusion | flops 10994688 | bytes 9744384 | tf_op jit(solution)/shard_map/while/body/eval_jaxpr/reduce_sum | solution.py:86
  198.3 3.0 %fusion.80 = f32[4,2,384,128]{2,3,1,0:T(8,128)S(1)} fusion(f32[4,2,384,4]{2,1,3,0:T(2,128)} %copy.67, bf16[4,2,384,4,128]{2,4,3,1,0:T(8,128)(2,1)} %get-tuple-element.277, bf16[1,4,128,4,128]{2,4,1,3,0:T(8,128)(2,1)S(1)} %copy.68), kind=kOutput, calls=%fused_computation.5.clone.1 | convolution fusion | flops 405405696 | bytes 5292032 | tf_op jit(solution)/shard_map/while/body/eval_jaxpr/hmqgk,gkhc->hmqgc/dot_general | solution.py:87
  208.1 3.3 %fusion.77 = (f32[4,2,384,4]{2,3,1,0:T(4,128)S(1)}, f32[4,2,384]{2,1,0:T(2,128)S(1)}, bf16[4,2,384,4,128]{2,4,3,1,0:T(8,128)(2,1)}) fusion(f32[4,2,4,128,384]{4,3,2,1,0:T(8,128)S(1)} %get-tuple-element.270, f32[4,2,384,4]{2,3,1,0:T(4,128)S(1)} %get-tuple-element.271, pred[384,4,128]{0,2,1:T(8,128)(4,1)S(1)} %broadcast_compare_fusion.2), kind=kLoop, calls=%fused_computation.9.clone.1 | loop fusion | flops 10994688 | bytes 9744384 | tf_op jit(solution)/shard_map/while/body/eval_jaxpr/reduce_sum | solution.py:86
  214.3 3.0 %fusion.80 = f32[4,2,384,128]{2,3,1,0:T(8,128)S(1)} fusion(f32[4,2,384,4]{2,1,3,0:T(2,128)} %copy.67, bf16[4,2,384,4,128]{2,4,3,1,0:T(8,128)(2,1)} %get-tuple-element.277, bf16[1,4,128,4,128]{2,4,1,3,0:T(8,128)(2,1)S(1)} %copy.68), kind=kOutput, calls=%fused_computation.5.clone.1 | convolution fusion | flops 405405696 | bytes 5292032 | tf_op jit(solution)/shard_map/while/body/eval_jaxpr/hmqgk,gkhc->hmqgc/dot_general | solution.py:87
  224.1 3.3 %fusion.77 = (f32[4,2,384,4]{2,3,1,0:T(4,128)S(1)}, f32[4,2,384]{2,1,0:T(2,128)S(1)}, bf16[4,2,384,4,128]{2,4,3,1,0:T(8,128)(2,1)}) fusion(f32[4,2,4,128,384]{4,3,2,1,0:T(8,128)S(1)} %get-tuple-element.270, f32[4,2,384,4]{2,3,1,0:T(4,128)S(1)} %get-tuple-element.271, pred[384,4,128]{0,2,1:T(8,128)(4,1)S(1)} %broadcast_compare_fusion.2), kind=kLoop, calls=%fused_computation.9.clone.1 | loop fusion | flops 10994688 | bytes 9744384 | tf_op jit(solution)/shard_map/while/body/eval_jaxpr/reduce_sum | solution.py:86
  230.4 3.0 %fusion.80 = f32[4,2,384,128]{2,3,1,0:T(8,128)S(1)} fusion(f32[4,2,384,4]{2,1,3,0:T(2,128)} %copy.67, bf16[4,2,384,4,128]{2,4,3,1,0:T(8,128)(2,1)} %get-tuple-element.277, bf16[1,4,128,4,128]{2,4,1,3,0:T(8,128)(2,1)S(1)} %copy.68), kind=kOutput, calls=%fused_computation.5.clone.1 | convolution fusion | flops 405405696 | bytes 5292032 | tf_op jit(solution)/shard_map/while/body/eval_jaxpr/hmqgk,gkhc->hmqgc/dot_general | solution.py:87
  244.2 3.5 %all-to-all-start.1 = ((bf16[8,50,512]{2,1,0:T(8,128)(2,1)}), bf16[8,50,512]{2,1,0:T(8,128)(2,1)S(1)}, u32[]{:S(2)}, u32[]{:S(2)}) async-start(bf16[8,50,512]{2,1,0:T(8,128)(2,1)} %all_to_all.19), calls=%async_computation.3 | async-start | bytes 917504 | tf_op jit(solution)/shard_map/all_to_all | solution.py:151
  248.0 13.6 %all-to-all-done.1 = bf16[8,50,512]{2,1,0:T(8,128)(2,1)S(1)} async-done(((bf16[8,50,512]{2,1,0:T(8,128)(2,1)}), bf16[8,50,512]{2,1,0:T(8,128)(2,1)S(1)}, u32[]{:S(2)}, u32[]{:S(2)}) %all-to-all-start.1) | async-done | bytes 409632 | tf_op jit(solution)/shard_map/all_to_all | solution.py:151
  266.6 4.7 %reduce-scatter.4.cloned.1.call-done = bf16[384,512]{1,0:T(8,128)(2,1)} async-done(((bf16[384,2048]{1,0:T(8,128)(2,1)}), bf16[384,512]{1,0:T(8,128)(2,1)}) %reduce-scatter.4.cloned.1.call-update) | async-done | bytes 393232 | tf_op jit(solution)/shard_map/reduce_scatter | solution.py:115
  (228 shorter events, 87.5 us)
Async XLA Ops:
  8.0 107.8 %copy-start = (bf16[1,512,2048]{2,1,0:T(8,128)(2,1)S(1)}, bf16[1,512,2048]{2,1,0:T(8,128)(2,1)}, u32[]{:S(2)}) copy-start(bf16[1,512,2048]{2,1,0:T(8,128)(2,1)} %param.30) | copy-start | bytes 6291460
  8.0 120.9 %all-gather.3.cloned.1.call-start = ((), (), s32[]{:S(2)}) async-start(), calls=%async_computation.5 | async-start | bytes 3538944 | tf_op jit(solution)/shard_map/all_gather | solution.py:64
  11.4 4.0 %copy-start.11 = (s32[160,2]{0,1:T(2,128)S(1)}, s32[160,2]{0,1:T(2,128)}, u32[]{:S(2)}) copy-start(s32[160,2]{0,1:T(2,128)} %param.26) | copy-start | bytes 3844
  11.7 8.7 %copy-start.1 = (bf16[160,2048]{1,0:T(8,128)(2,1)S(1)}, bf16[160,2048]{1,0:T(8,128)(2,1)}, u32[]{:S(2)}) copy-start(bf16[160,2048]{1,0:T(8,128)(2,1)} %param.24) | copy-start | bytes 1966084
  13.9 6.7 %copy-start.2 = (bf16[160,2048]{1,0:T(8,128)(2,1)S(1)}, bf16[160,2048]{1,0:T(8,128)(2,1)}, u32[]{:S(2)}) copy-start(bf16[160,2048]{1,0:T(8,128)(2,1)} %param.24) | copy-start | bytes 1966084
  13.9 6.7 %copy-start.10 = (f32[2048]{0:T(1024)S(1)}, f32[2048]{0:T(1024)}, u32[]{:S(2)}) copy-start(f32[2048]{0:T(1024)} %param.25) | copy-start | bytes 24580
  14.7 121.0 %all-gather.5.cloned.1.call-start = ((), (), s32[]{:S(2)}) async-start(), calls=%async_computation.6 | async-start | bytes 3538944 | tf_op jit(solution)/shard_map/all_gather | solution.py:65
  15.4 226.8 %reduce-scatter.6.cloned.1.call-start = ((), (), s32[]{:S(2)}) async-start(), calls=%async_computation.8 | async-start | bytes 2048000 | tf_op jit(solution)/shard_map/reduce_scatter | solution.py:144
  121.3 143.7 %reduce-scatter.8.cloned.1.call-start = ((), (), s32[]{:S(2)}) async-start(), calls=%async_computation.9 | async-start | bytes 819200 | tf_op jit(solution)/shard_map/reduce_scatter | solution.py:147
  127.6 143.7 %reduce-scatter.4.cloned.1.call-start = ((), (), s32[]{:S(2)}) async-start(), calls=%async_computation.7 | async-start | bytes 1966080 | tf_op jit(solution)/shard_map/reduce_scatter | solution.py:115
  141.3 7.4 %copy-start.4 = (f32[4,2,384]{2,1,0:T(2,128)}, f32[4,2,384]{2,1,0:T(2,128)S(1)}, u32[]{:S(2)}) copy-start(f32[4,2,384]{2,1,0:T(2,128)S(1)} %get-tuple-element.292) | copy-start | bytes 36868 | tf_op jit(solution)/shard_map/while
  156.0 7.2 %copy-start.4 = (f32[4,2,384]{2,1,0:T(2,128)}, f32[4,2,384]{2,1,0:T(2,128)S(1)}, u32[]{:S(2)}) copy-start(f32[4,2,384]{2,1,0:T(2,128)S(1)} %get-tuple-element.292) | copy-start | bytes 36868 | tf_op jit(solution)/shard_map/while
  172.1 7.2 %copy-start.4 = (f32[4,2,384]{2,1,0:T(2,128)}, f32[4,2,384]{2,1,0:T(2,128)S(1)}, u32[]{:S(2)}) copy-start(f32[4,2,384]{2,1,0:T(2,128)S(1)} %get-tuple-element.292) | copy-start | bytes 36868 | tf_op jit(solution)/shard_map/while
  182.3 3.0 %copy-start.5 = (f32[4,2,384]{2,1,0:T(2,128)S(1)}, f32[4,2,384]{2,1,0:T(2,128)}, u32[]{:S(2)}) copy-start(f32[4,2,384]{2,1,0:T(2,128)} %copy-done.4) | copy-start | bytes 36868 | tf_op jit(solution)/shard_map/while
  182.3 3.0 %copy-start.6 = (f32[4,2,384]{2,1,0:T(2,128)S(1)}, f32[4,2,384]{2,1,0:T(2,128)}, u32[]{:S(2)}) copy-start(f32[4,2,384]{2,1,0:T(2,128)} %get-tuple-element.274) | copy-start | bytes 36868 | tf_op jit(solution)/shard_map/while
  182.3 3.0 %copy-start.7 = (f32[4,2,384]{2,1,0:T(2,128)S(1)}, f32[4,2,384]{2,1,0:T(2,128)}, u32[]{:S(2)}) copy-start(f32[4,2,384]{2,1,0:T(2,128)} %get-tuple-element.293) | copy-start | bytes 36868 | tf_op jit(solution)/shard_map/while
  188.1 7.2 %copy-start.4 = (f32[4,2,384]{2,1,0:T(2,128)}, f32[4,2,384]{2,1,0:T(2,128)S(1)}, u32[]{:S(2)}) copy-start(f32[4,2,384]{2,1,0:T(2,128)S(1)} %get-tuple-element.292) | copy-start | bytes 36868 | tf_op jit(solution)/shard_map/while
  204.1 7.2 %copy-start.4 = (f32[4,2,384]{2,1,0:T(2,128)}, f32[4,2,384]{2,1,0:T(2,128)S(1)}, u32[]{:S(2)}) copy-start(f32[4,2,384]{2,1,0:T(2,128)S(1)} %get-tuple-element.292) | copy-start | bytes 36868 | tf_op jit(solution)/shard_map/while
  214.3 3.0 %copy-start.5 = (f32[4,2,384]{2,1,0:T(2,128)S(1)}, f32[4,2,384]{2,1,0:T(2,128)}, u32[]{:S(2)}) copy-start(f32[4,2,384]{2,1,0:T(2,128)} %copy-done.4) | copy-start | bytes 36868 | tf_op jit(solution)/shard_map/while
  214.3 3.0 %copy-start.6 = (f32[4,2,384]{2,1,0:T(2,128)S(1)}, f32[4,2,384]{2,1,0:T(2,128)}, u32[]{:S(2)}) copy-start(f32[4,2,384]{2,1,0:T(2,128)} %get-tuple-element.274) | copy-start | bytes 36868 | tf_op jit(solution)/shard_map/while
  220.1 7.2 %copy-start.4 = (f32[4,2,384]{2,1,0:T(2,128)}, f32[4,2,384]{2,1,0:T(2,128)S(1)}, u32[]{:S(2)}) copy-start(f32[4,2,384]{2,1,0:T(2,128)S(1)} %get-tuple-element.292) | copy-start | bytes 36868 | tf_op jit(solution)/shard_map/while
  242.2 5.5 %copy-start.9 = (s32[160,2]{1,0:T(8,128)S(1)}, s32[160,2]{1,0:T(8,128)}, u32[]{:S(2)}) copy-start(s32[160,2]{1,0:T(8,128)} %get-tuple-element.202) | copy-start | bytes 3844
  242.2 5.6 %copy-start.12 = (f32[160,2]{0,1:T(2,128)S(1)}, f32[160,2]{0,1:T(2,128)}, u32[]{:S(2)}) copy-start(f32[160,2]{0,1:T(2,128)} %param.27) | copy-start | bytes 3844
  244.2 17.3 %all-to-all-start.1 = ((bf16[8,50,512]{2,1,0:T(8,128)(2,1)}), bf16[8,50,512]{2,1,0:T(8,128)(2,1)S(1)}, u32[]{:S(2)}, u32[]{:S(2)}) async-start(bf16[8,50,512]{2,1,0:T(8,128)(2,1)} %all_to_all.19), calls=%async_computation.3 | async-start | bytes 917504 | tf_op jit(solution)/shard_map/all_to_all | solution.py:151
  (22 other events, 59.9 us)
Sparse Core Ops, SparseCore 0:
  14.8 60.2 all-gather.2
  76.7 43.6 all-gather.4
Sparse Core Ops, SparseCore 1:
  121.4 29.5 reduce-scatter.5
  153.7 25.6 reduce-scatter.7
  242.3 28.9 reduce-scatter.3
where the time goes:
time: 281 us; the launch traced here: 279 us
  blocking collectives  79.5 us (28%)
  local copies, waits for them, and re-layouts  60.6 us (22%)
  other arithmetic  51.9 us (18%)
  matrix products  43.2 us (15%)
  waiting for transfers between devices  19.1 us (7%)
  between operations  16 us (6%)
  loops' own time  4.69 us (2%)
  starting transfers between devices  3.88 us (1%)
    all_to_all x1, blocking collectives, local(): lax.all_to_all(outgoing, 'ep', split_axis=0, concat_axis=0, tiled=True)  79.5 us
    dynamic_slice x24, local copies, waits for them, and re-layouts, local(): lax.scan(one_group, zero_init, (grouped_keys, grouped_values, jnp.arange(...  20.7 us
    reduce_sum x6, other arithmetic, one_group(): block_sum = jnp.sum(weights, axis=-1)  19.7 us
    dot_general x6, matrix products, one_group(): jnp.einsum('hmqgk,gkhc->hmqgc', weights.astype(jnp.bfloat16), block_value...  17.8 us
    add x6, other arithmetic, one_group(): run_out * old_scale[..., None]  15.1 us
    all_to_all x1, waiting for transfers between devices, local(): lax.all_to_all(expert_sum.astype(jnp.bfloat16), 'ep', split_axis=0, conca...  13.6 us
    dot_general x6, matrix products, one_group(): jnp.einsum('qhmd,gkhmd->hmqgk', rot_queries, block_keys, preferred_elemen...  7.55 us
    reshape x1, local copies, waits for them, and re-layouts, local(): piece_keys.reshape(group_count, group_size, KEY_BLOCK, local_heads, 2, he...  6.78 us
  transfers between devices with their start and end apart: 6, of which 2 were waited for; matrix products, arithmetic and copies ran while one was open for 50% of the time, Pallas kernels for 0%

commit v1 on v0

--- a/solution.py
+++ b/solution.py
@@ -1,6 +1,10 @@
+import functools
+
 import jax
 import jax.numpy as jnp
 from jax import lax
+from jax.experimental import pallas as pl
+from jax.experimental.pallas import tpu as pltpu
 from jax.sharding import PartitionSpec as P
 
 TOP_K = 2
@@ -26,24 +30,7 @@
     )
 
 
-def local(
-    query_pairs,
-    key_pairs,
-    value_rows,
-    head_lambda,
-    head_gain,
-    out_weight,
-    moe_input,
-    ffn_gain,
-    routes,
-    route_weight,
-    gate_weight,
-    up_weight,
-    down_weight,
-    shared_gate,
-    shared_up,
-    shared_down,
-):
+def generic_attention(query_pairs, key_pairs, value_rows, head_lambda, head_gain, out_weight):
     local_rows = query_pairs.shape[0]
     local_heads = head_lambda.shape[0]
     head_size = query_pairs.shape[1] // (2 * local_heads)
@@ -115,23 +102,306 @@
     attn_out = lax.psum_scatter(
         mixer_terms.astype(jnp.bfloat16), "tp", scatter_dimension=1, tiled=True
     )
+    return attn_out
+
+
+MESH = pl.DeviceIdType.MESH
+f32, bf16 = jnp.float32, jnp.bfloat16
+
+
+def rotate_kernel(head_size, scale, q_ref, k_ref, cos_ref, sin_ref, rq_ref, rk_ref):
+    heads, _, width = rq_ref.shape
+    half = head_size // 2
+    lane = lax.broadcasted_iota(jnp.int32, (q_ref.shape[0], width), 1)
+    front = lane % head_size < half
+    cosine, sine = cos_ref[...], sin_ref[...]
+    for source, target, factor in ((q_ref, rq_ref, scale), (k_ref, rk_ref, 1.0)):
+        for h in range(heads):
+            x = source[:, h * width : (h + 1) * width].astype(f32)
+            partner = jnp.where(front, pltpu.roll(x, width - half, 1), pltpu.roll(x, half, 1))
+            turned = (x * cosine + partner * sine).astype(bf16)
+            target[h] = turned if factor == 1.0 else turned * jnp.asarray(factor, bf16)
+
+
+def attention_kernel(
+    n, heads, lam_ref, gain_ref, rq_ref, rk_ref, v_ref, w_ref, out_ref,
+    q_buf, k_buf, v_buf, vt_buf, hn_send, hn_buf, w_buf, acc, m_buf, l_buf,
+    q_ss, q_rs, k_ss, k_rs, v_ss, v_rs, fk_ss, fk_rs, fv_ss, fv_rs, h_ss, h_rs, loc, w_sem,
+):
+    me = lax.axis_index("ep")
+    g = n // heads
+    my_head, my_core = me // g, me % g
+    rows = rk_ref.shape[1]
+    sub = rows // g
+    width = rk_ref.shape[2]
+    vw = v_buf.shape[2]
+
+    barrier = pltpu.get_barrier_semaphore()
+    for step in range(1, n):
+        pl.semaphore_signal(barrier, inc=1, device_id={"ep": lax.rem(me + step, n)}, device_id_type=MESH)
+    w_copy = pltpu.make_async_copy(w_ref, w_buf, w_sem)
+    w_copy.start()
+
+    def q_src(dest):
+        start = pl.multiple_of(((dest % g + me) % g) * sub, sub)
+        return rq_ref.at[dest // g, pl.ds(start, sub), :]
+
+    def v_src(dest):
+        return v_ref.at[:, pl.ds(pl.multiple_of((dest // g) * vw, vw), vw)]
+
+    own = (
+        pltpu.make_async_copy(q_src(me), q_buf.at[me], loc.at[0]),
+        pltpu.make_async_copy(rk_ref.at[my_head], k_buf.at[me], loc.at[1]),
+        pltpu.make_async_copy(v_src(me), v_buf.at[me], loc.at[2]),
+    )
+    for copy in own:
+        copy.start()
+    pl.semaphore_wait(barrier, n - 1)
+
+    def q_copy(dest):
+        return pltpu.make_async_remote_copy(
+            q_src(dest), q_buf.at[me], q_ss.at[dest], q_rs.at[me],
+            device_id={"ep": dest}, device_id_type=MESH)
+
+    def k_copy(dest):
+        return pltpu.make_async_remote_copy(
+            rk_ref.at[dest // g], k_buf.at[me], k_ss.at[dest], k_rs.at[me],
+            device_id={"ep": dest}, device_id_type=MESH)
+
+    def v_copy(dest):
+        return pltpu.make_async_remote_copy(
+            v_src(dest), v_buf.at[me], v_ss.at[dest], v_rs.at[me],
+            device_id={"ep": dest}, device_id_type=MESH)
+
+    for step in range(1, n):
+        dest = lax.rem(me + step, n)
+        if step % g == 0:
+            k_copy(dest).start()
+            v_copy(dest).start()
+        q_copy(dest).start()
+
+    def mate(step):
+        return my_head * g + lax.rem(my_core + step, g)
+
+    def recv(buf, sem, source):
+        return pltpu.make_async_remote_copy(
+            buf.at[source], buf.at[source], sem.at[source], sem.at[source],
+            device_id={"ep": lax.rem(me + 1, n)}, device_id_type=MESH)
+
+    def forward(source, step):
+        to = mate(step)
+        return (
+            pltpu.make_async_remote_copy(
+                k_buf.at[source], k_buf.at[source], fk_ss.at[source, step], fk_rs.at[source],
+                device_id={"ep": to}, device_id_type=MESH),
+            pltpu.make_async_remote_copy(
+                v_buf.at[source], v_buf.at[source], fv_ss.at[source, step], fv_rs.at[source],
+                device_id={"ep": to}, device_id_type=MESH),
+        )
+
+    for copy in own:
+        copy.wait()
+
+    lam = lam_ref[my_head]
+    gain = gain_ref[...]
+    key_row = lax.broadcasted_iota(jnp.int32, (rows, g_cols(sub)), 0)
+    query_col = lax.broadcasted_iota(jnp.int32, (rows, g_cols(sub)), 1) % sub
+    lane = lax.broadcasted_iota(jnp.int32, (sub, width), 1)
+
+    def group(p, _):
+        direct = p * g + my_core
+
+        @pl.when(direct != me)
+        def _():
+            recv(k_buf, k_rs, direct).wait_recv()
+            recv(v_buf, v_rs, direct).wait_recv()
+
+        for step in range(1, g):
+            for copy in forward(direct, step):
+                copy.start()
+        for step in range(1, g):
+            other = p * g + lax.rem(my_core + step, g)
+            recv(k_buf, fk_rs, other).wait_recv()
+            recv(v_buf, fv_rs, other).wait_recv()
+
+        def member(c, _):
+            e = p * g + c
+            vt_buf[e] = v_buf[e].astype(f32).T.astype(bf16)
+
+            @pl.when(e != me)
+            def _():
+                recv(q_buf, q_rs, e).wait_recv()
+
+            q = q_buf[e]
+            zero = jnp.zeros_like(q)
+            stacked = jnp.concatenate(
+                [jnp.where(lane < width // 2, q, zero), jnp.where(lane < width // 2, zero, q)], axis=0)
+            q_start = ((my_core + e) % g) * sub
+
+            def scores_of(j):
+                return lax.dot_general(
+                    k_buf[j], stacked, (((1,), (1,)), ((), ())), preferred_element_type=f32)
+
+            s = jnp.where(key_row <= query_col + q_start, scores_of(e), masked_low)
+            m = jnp.max(s, axis=0, keepdims=True)
+            weights = jnp.exp(s - m)
+            l_buf[...] = jnp.sum(weights, axis=0, keepdims=True)
+            m_buf[...] = m
+            acc[...] = jnp.dot(vt_buf[e], weights.astype(bf16), preferred_element_type=f32)
+
+            def block(j, _):
+                s = scores_of(j)
+                old = m_buf[...]
+                m = jnp.maximum(old, jnp.max(s, axis=0, keepdims=True))
+                weights = jnp.exp(s - m)
+                scale = jnp.exp(old - m)
+                l_buf[...] = l_buf[...] * scale + jnp.sum(weights, axis=0, keepdims=True)
+                m_buf[...] = m
+                acc[...] = acc[...] * scale + jnp.dot(
+                    vt_buf[j], weights.astype(bf16), preferred_element_type=f32)
+                return 0
+
+            lax.fori_loop(0, e, block, 0)
+            a = (acc[...] / l_buf[...]).T
+            diff = a[:sub] - lam * a[sub:]
+            inverse = lax.rsqrt(jnp.mean(diff * diff, axis=-1, keepdims=True) + norm_eps)
+            hn_send[e] = (diff * inverse * gain).astype(bf16)
+
+            @pl.when(e != me)
+            def _():
+                hn_copy(e).start()
+
+            return 0
+
+        lax.fori_loop(0, g, member, 0)
+        return 0
+
+    def hn_copy(dest):
+        return pltpu.make_async_remote_copy(
+            hn_send.at[dest], hn_buf.at[me], h_ss.at[dest], h_rs.at[me],
+            device_id={"ep": dest}, device_id_type=MESH)
+
+    lax.fori_loop(0, heads, group, 0)
+    hn_buf[me] = hn_send[me]
+    for step in range(1, n):
+        source = lax.rem(me + step, n)
+        recv(hn_buf, h_rs, source).wait_recv()
+    w_copy.wait()
+    for part in range(g):
+        normed = jnp.concatenate(
+            [hn_buf[h * g + lax.rem(part + me, g)] for h in range(heads)], axis=1)
+        out_ref[part * sub : (part + 1) * sub, :] = jnp.dot(
+            normed, w_buf[...], preferred_element_type=f32).astype(bf16)
+    for step in range(1, n):
+        dest = lax.rem(me + step, n)
+        if step % g == 0:
+            k_copy(dest).wait_send()
+            v_copy(dest).wait_send()
+        q_copy(dest).wait_send()
+        hn_copy(dest).wait_send()
+    for p in range(heads):
+        for step in range(1, g):
+            for copy in forward(p * g + my_core, step):
+                copy.wait_send()
+
+
+def g_cols(sub):
+    return 2 * sub
+
+
+def exchange_attention(query_pairs, key_pairs, value_rows, head_lambda, head_gain, out_weight):
+    n = lax.axis_size("ep")
+    rows = query_pairs.shape[0]
+    heads = head_lambda.shape[0]
+    width = query_pairs.shape[1] // heads
+    head_size = width // 2
+    vw = value_rows.shape[1] // heads
+    sub = rows * heads // n
+    positions = lax.axis_index("ep") * rows + jnp.arange(rows, dtype=jnp.int32)
+    half = head_size // 2
+    frequency = theta_base ** (-(jnp.arange(half, dtype=f32) * 2.0) / head_size)
+    angles = positions.astype(f32)[:, None] * frequency[None, :]
+    cosine, sine = jnp.cos(angles), jnp.sin(angles)
+    cosines = jnp.concatenate([cosine] * 4, axis=1)
+    sines = jnp.concatenate([-sine, sine] * 2, axis=1)
+    turned = jax.ShapeDtypeStruct((heads, rows, width), bf16)
+    rq, rk = pl.pallas_call(
+        functools.partial(rotate_kernel, head_size, head_size ** (-0.5)),
+        out_shape=(turned, turned),
+        name="rotate",
+    )(query_pairs, key_pairs, cosines, sines)
+    any_spec = pl.BlockSpec(memory_space=pl.ANY)
+    vmem = pl.BlockSpec(memory_space=pltpu.VMEM)
+    dma = pltpu.SemaphoreType.DMA
+    g = n // heads
+    terms = pl.pallas_call(
+        functools.partial(attention_kernel, n, heads),
+        out_shape=jax.ShapeDtypeStruct((rows, out_weight.shape[1]), bf16),
+        in_specs=[pl.BlockSpec(memory_space=pltpu.SMEM), vmem, any_spec, any_spec, any_spec, any_spec],
+        out_specs=vmem,
+        scratch_shapes=[
+            pltpu.VMEM((n, sub, width), bf16),
+            pltpu.VMEM((n, rows, width), bf16),
+            pltpu.VMEM((n, rows, vw), bf16),
+            pltpu.VMEM((n, vw, rows), bf16),
+            pltpu.VMEM((n, sub, vw), bf16),
+            pltpu.VMEM((n, sub, vw), bf16),
+            pltpu.VMEM(out_weight.shape, bf16),
+            pltpu.VMEM((vw, 2 * sub), f32),
+            pltpu.VMEM((1, 2 * sub), f32),
+            pltpu.VMEM((1, 2 * sub), f32),
+            dma((n,)), dma((n,)), dma((n,)), dma((n,)), dma((n,)), dma((n,)),
+            dma((n, g)), dma((n,)), dma((n, g)), dma((n,)),
+            dma((n,)), dma((n,)), dma((3,)), dma(()),
+        ],
+        compiler_params=pltpu.CompilerParams(
+            collective_id=0, has_side_effects=True, vmem_limit_bytes=40 * 2**20),
+        cost_estimate=pl.CostEstimate(flops=20 * 10**9, bytes_accessed=8 * 2**20, transcendentals=5 * 10**6),
+        name="attention",
+    )(head_lambda, head_gain.reshape(1, vw), rq, rk, value_rows, out_weight)
+    return lax.psum_scatter(terms, "tp", scatter_dimension=1, tiled=True)
+
+
+def local(
+    query_pairs,
+    key_pairs,
+    value_rows,
+    head_lambda,
+    head_gain,
+    out_weight,
+    moe_input,
+    ffn_gain,
+    routes,
+    route_weight,
+    gate_weight,
+    up_weight,
+    down_weight,
+    shared_gate,
+    shared_up,
+    shared_down,
+):
+    n = lax.axis_size("ep")
+    heads = head_lambda.shape[0]
+    rows = query_pairs.shape[0]
+    fits = n % heads == 0 and n // heads > 1 and (rows * heads) % (n * 64) == 0
+    attention = exchange_attention if fits else generic_attention
+    attn_out = attention(query_pairs, key_pairs, value_rows, head_lambda, head_gain, out_weight)
     row_values = moe_input.astype(jnp.float32)
     inverse_norm = lax.rsqrt(jnp.mean(row_values * row_values, axis=-1, keepdims=True) + norm_eps)
     normed = (row_values * inverse_norm * ffn_gain).astype(jnp.bfloat16)
-    token_rows = normed.shape[0]
-    experts = lax.axis_size("ep")
-    capacity = token_rows * TOP_K * 5 // (4 * experts)
-    flat_routes = routes.reshape(-1)
-    onehot = (flat_routes[:, None] == jnp.arange(experts, dtype=jnp.int32)).astype(jnp.int32)
-    slot_rank = jnp.sum((jnp.cumsum(onehot, axis=0) - 1) * onehot, axis=-1)
-    slot_index = flat_routes * capacity + slot_rank
-    token_index = jnp.arange(token_rows * TOP_K, dtype=jnp.int32) // TOP_K
-    slot_rows = (
-        jnp.full((experts * capacity,), token_rows, jnp.int32).at[slot_index].set(token_index)
-    )
-    padded = jnp.concatenate([normed, jnp.zeros((1, normed.shape[1]), jnp.bfloat16)], axis=0)
-    outgoing = padded[slot_rows]
-    arrived = lax.all_to_all(outgoing, "ep", split_axis=0, concat_axis=0, tiled=True)
+    tokens, model = normed.shape
+    n_tp = lax.axis_size("tp")
+    capacity = tokens * TOP_K * 5 // (4 * n)
+    part = lax.dynamic_slice_in_dim(normed, lax.axis_index("tp") * (model // n_tp), model // n_tp, axis=1)
+    gathered = lax.all_gather(part, ("ep", "tp"), axis=0, tiled=False)
+    gathered = gathered.reshape(n, n_tp, tokens, model // n_tp)
+    all_routes = lax.all_gather(routes, "ep", axis=0, tiled=False)
+    hit = jnp.any(all_routes == lax.axis_index("ep"), axis=-1)
+    lower = jnp.tril(jnp.ones((tokens, tokens), bf16))
+    rank = jnp.dot(hit.astype(bf16), lower.T, preferred_element_type=f32).astype(jnp.int32) - 1
+    select = (hit[:, None, :] & (rank[:, None, :] == jnp.arange(capacity, dtype=jnp.int32)[None, :, None])).astype(bf16)
+    arrived = jnp.einsum("bst,bhtd->bshd", select, gathered, preferred_element_type=f32).astype(bf16)
+    arrived = arrived.reshape(n * capacity, model)
     gate_part = jnp.dot(arrived, gate_weight[0], preferred_element_type=jnp.float32)
     up_part = jnp.dot(arrived, up_weight[0], preferred_element_type=jnp.float32)
     hidden = (jax.nn.silu(gate_part) * up_part).astype(jnp.bfloat16)
@@ -140,21 +410,20 @@
     shared_lifted = jnp.dot(normed, shared_up, preferred_element_type=jnp.float32)
     shared_hidden = (jax.nn.silu(shared_gated) * shared_lifted).astype(jnp.bfloat16)
     shared_terms = jnp.dot(shared_hidden, shared_down, preferred_element_type=jnp.float32)
-    expert_sum, shared_sum = (
-        lax.psum_scatter(
-            expert_terms.astype(jnp.bfloat16), "tp", scatter_dimension=1, tiled=True
-        ).astype(jnp.float32),
-        lax.psum_scatter(
-            shared_terms.astype(jnp.bfloat16), "tp", scatter_dimension=1, tiled=True
-        ).astype(jnp.float32),
-    )
-    returned = lax.all_to_all(
-        expert_sum.astype(jnp.bfloat16), "ep", split_axis=0, concat_axis=0, tiled=True
-    )
-    picked = returned[slot_index.reshape(token_rows, TOP_K)]
-    moe_out = (
-        jnp.sum(route_weight[..., None] * picked.astype(jnp.float32), axis=1) + shared_sum
-    ).astype(jnp.bfloat16)
+    both = jnp.concatenate([expert_terms.astype(bf16), shared_terms.astype(bf16)], axis=0)
+    sums = lax.psum_scatter(both, "tp", scatter_dimension=1, tiled=True)
+    expert_sum, shared_sum = sums[: n * capacity], sums[n * capacity :].astype(f32)
+    returned = lax.all_to_all(expert_sum, "ep", split_axis=0, concat_axis=0, tiled=True)
+    onehot = (routes[:, :, None] == jnp.arange(n, dtype=jnp.int32)).astype(bf16)
+    named = jnp.sum(onehot, axis=1)
+    ranks = jnp.dot(lower, named, preferred_element_type=f32) - 1.0
+    slots = jnp.sum(onehot.astype(f32) * (ranks[:, None, :] + jnp.arange(n, dtype=f32) * capacity), axis=-1)
+    moe_out = shared_sum
+    for k in range(TOP_K):
+        place = (slots[:, k : k + 1].astype(jnp.int32) == jnp.arange(n * capacity, dtype=jnp.int32)).astype(bf16)
+        picked = jnp.dot(place, returned, preferred_element_type=f32)
+        moe_out = moe_out + route_weight[:, k : k + 1] * picked
+    moe_out = moe_out.astype(bf16)
     return (attn_out, moe_out)
 
 

time: 281 us -> 198 us (0.70)
  blocking collectives: 79.5 us -> 14.5 us
  waiting for transfers between devices: 19.1 us -> 70.2 us
  local copies, waits for them, and re-layouts: 60.6 us -> 10.4 us
  Pallas kernels: 0 us -> 46.5 us
  other arithmetic: 51.9 us -> 7.86 us
  matrix products: 43.2 us -> 19.2 us
  starting transfers between devices: 3.88 us -> 14.4 us
  loops' own time: 4.69 us -> 0 us
    all_to_all x1 -> x0, blocking collectives: 79.5 us -> none  [local(): lax.all_to_all(outgoing, 'ep', split_axis=0, concat_axis=0, tiled=True)]
    all_gather x2 -> x1, waiting for transfers between devices: 0.02 us -> 47.9 us  [local(): gathered = lax.all_gather(part, ('ep', 'tp'), axis=0, tiled=False)]
    pallas_call x0 -> x2, Pallas kernels: none -> 46.5 us  [the longest x1 43.9 us: exchange_attention(): pl.pallas_call(functools.partial(attention_kernel, n, heads), out_shape=j...]
    reduce_sum x15 -> x2, other arithmetic: 24.7 us -> 0.08 us  [the longest x1 0.07 us: local(): jnp.sum(onehot.astype(f32) * (ranks[:, None, :] + jnp.arange(n, dtype=f32...]
    dot_general x13 -> x5, matrix products: 27.5 us -> 5.76 us  [the longest x1 3.33 us: local(): jnp.einsum('bst,bhtd->bshd', select, gathered, preferred_element_type=f32)]
    dynamic_slice x24 -> x1, local copies, waits for them, and re-layouts: 20.7 us -> 0.69 us  [local(): lax.dynamic_slice_in_dim(normed, lax.axis_index('tp') * (model // n_tp),...]
    reshape x4 -> x0, local copies, waits for them, and re-layouts: 15.7 us -> none  [the longest x1 6.78 us: local(): piece_keys.reshape(group_count, group_size, KEY_BLOCK, local_heads, 2, he...]
    add x24 -> x0, other arithmetic: 15.4 us -> none  [the longest x6 15.1 us: one_group(): run_out * old_scale[..., None]]
  transfers between devices with their start and end apart: 6 -> 4, of which waited for: 2 -> 3; matrix products, arithmetic and copies ran while one was open for 50% -> 6% of each run, Pallas kernels for 0% -> 24%
where the time goes in v1:
time: 198 us; the launch traced here: 197 us
  waiting for transfers between devices  70.2 us (35%)
  Pallas kernels  46.5 us (23%)
  matrix products  19.2 us (10%)
  blocking collectives  14.5 us (7%)
  starting transfers between devices  14.4 us (7%)
  between operations  13.9 us (7%)
  local copies, waits for them, and re-layouts  10.4 us (5%)
  other arithmetic  7.86 us (4%)
    all_gather x1, waiting for transfers between devices, local(): gathered = lax.all_gather(part, ('ep', 'tp'), axis=0, tiled=False)  47.9 us
    pallas_call x1, Pallas kernels, exchange_attention(): pl.pallas_call(functools.partial(attention_kernel, n, heads), out_shape=j...  43.9 us
    all_gather x1, blocking collectives, local(): all_routes = lax.all_gather(routes, 'ep', axis=0, tiled=False)  14.5 us
    all_to_all x1, starting transfers between devices, local(): lax.all_to_all(expert_sum, 'ep', split_axis=0, concat_axis=0, tiled=True)  14.3 us
    all_to_all x1, waiting for transfers between devices, local(): lax.all_to_all(expert_sum, 'ep', split_axis=0, concat_axis=0, tiled=True)  13.7 us
    reduce_scatter x1, waiting for transfers between devices, exchange_attention(): return lax.psum_scatter(terms, 'tp', scatter_dimension=1, tiled=True)  8.57 us
    unnamed x25, local copies, waits for them, and re-layouts  6.84 us
    dot_general x1, matrix products, local(): jnp.dot(hidden, down_weight[0], preferred_element_type=jnp.float32)  5.39 us
  transfers between devices with their start and end apart: 4, of which 3 were waited for; matrix products, arithmetic and copies ran while one was open for 6% of the time, Pallas kernels for 24%

profile of v1, /device:TPU:0, one launch (start us, length us, event | category | flops | bytes accessed | tf_op | source)
XLA Modules:
  0.0 197.1 jit_solution(17618008888724852846)
XLA Ops:
  7.2 1.4 fusion.5
  8.7 1.3 fusion.7
  10.8 14.5 %all-gather.2 = s32[8,160,2]{1,2,0:T(2,128)S(1)} all-gather(s32[1,160,2]{1,2,0:T(2,128)S(1)} %bitcast.47), channel_id=2, replica_groups=mesh['ep'=8,'tp'=4] {'ep'}, dimensions={0}, use_global_device_ids=true | all-gather | bytes 11520 | tf_op jit(solution)/shard_map/all_gather | solution.py:398
  25.4 2.9 %fusion.56 = f32[160,512]{1,0:T(8,128)} fusion(bf16[160,2048]{1,0:T(8,128)(2,1)S(1)} %fusion.7, bf16[2048,512]{1,0:T(8,128)(2,1)} %param.29), kind=kOutput, calls=%fused_computation.76 | convolution fusion | flops 335544320 | bytes 3080192 | tf_op jit(solution)/shard_map/dot_general | solution.py:409
  28.3 3.3 %convolution_convert_fusion.1 = bf16[160,2048]{1,0:T(8,128)(2,1)S(1)} fusion(bf16[512,2048]{1,0:T(8,128)(2,1)} %param.31, bf16[160,2048]{1,0:T(8,128)(2,1)S(1)} %fusion.7, bf16[2048,512]{1,0:T(8,128)(2,1)} %param.30, f32[160,512]{1,0:T(8,128)} %fusion.56), kind=kOutput, calls=%fused_computation.1 | convolution fusion | flops 671907840 | bytes 5832704 | tf_op jit(solution)/shard_map/dot_general | solution.py:412
  31.6 47.9 %all-gather.5.cloned.1.call-done = bf16[5120,512]{1,0:T(8,128)(2,1)} async-done(((bf16[160,512]{1,0:T(8,128)(2,1)}), bf16[5120,512]{1,0:T(8,128)(2,1)}) %all-gather.5.cloned.1.call-update) | async-done | bytes 5242896 | tf_op jit(solution)/shard_map/all_gather | solution.py:396
  79.5 3.3 %convolution_convert_fusion.2 = bf16[8,50,4,512]{3,1,2,0:T(8,128)(2,1)S(1)} fusion(bf16[8,4,160,512]{3,2,1,0:T(8,128)(2,1)} %bitcast.43, s32[8,160]{1,0:T(8,128)S(1)} %fusion.19, pred[8,160]{1,0:T(8,128)(4,1)S(1)} %compare_reduce_fusion), kind=kOutput, calls=%fused_computation.8 | convolution fusion | flops 263091200 | bytes 6887680 | tf_op jit(solution)/shard_map/bst,bhtd->bshd/dot_general | solution.py:403
  84.1 1.2 copy-done.8
  85.6 1.9 fusion.3
  87.5 5.4 %convolution_convert_fusion = bf16[400,2048]{1,0:T(8,128)(2,1)} fusion(bf16[1,512,2048]{2,1,0:T(8,128)(2,1)S(1)} %copy-done, bf16[400,2048]{1,0:T(8,128)(2,1)} %bitcast.46, bf16[1,2048,512]{2,1,0:T(8,128)(2,1)} %param.27, f32[400,512]{1,0:T(8,128)} %fusion.3), kind=kOutput, calls=%fused_computation | convolution fusion | flops 1679769600 | bytes 8290304 | tf_op jit(solution)/shard_map/dot_general | solution.py:408
  92.9 3.0 %pad_maximum_fusion = bf16[560,2048]{1,0:T(8,128)(2,1)} fusion(bf16[160,2048]{1,0:T(8,128)(2,1)S(1)} %convolution_convert_fusion.1, bf16[400,2048]{1,0:T(8,128)(2,1)} %convolution_convert_fusion), kind=kLoop, calls=%fused_computation.2 | loop fusion | flops 4587520 | bytes 4587520 | tf_op jit(solution)/shard_map/concatenate | solution.py:413
  96.8 1.1 pad_maximum_fusion.1
  98.0 2.6 %rotate.1 = (bf16[4,384,128]{2,1,0:T(8,128)(2,1)}, bf16[4,384,128]{2,1,0:T(8,128)(2,1)}) custom-call(bf16[384,512]{1,0:T(8,128)(2,1)} %q_ref.1, bf16[384,512]{1,0:T(8,128)(2,1)} %k_ref.1, f32[384,128]{1,0:T(8,128)} %get-tuple-element.13.cos_ref, f32[384,128]{1,0:T(8,128)} %get-tuple-element.14.sin_ref), custom_call_target="tpu_custom_call" | custom-call | tf_op jit(solution)/shard_map/rotate/pallas_call | solution.py:328
  100.6 1.8 copy-done.2
  102.4 1.0 copy-done.4
  103.4 1.0 copy-done.5
  104.4 43.9 %attention.1 = bf16[384,2048]{1,0:T(8,128)(2,1)S(1)} custom-call(f32[4]{0:T(128)S(1)} %copy-done.6, f32[1,128]{1,0:T(1,128)S(1)} %bitcast.42, bf16[4,384,128]{2,1,0:T(8,128)(2,1)S(1)} %copy-done.4, bf16[4,384,128]{2,1,0:T(8,128)(2,1)S(1)} %copy-done.5, bf16[384,512]{1,0:T(8,128)(2,1)S(1)} %copy-done.3, bf16[512,2048]{1,0:T(8,128)(2,1)S(1)} %copy-done.2), custom_call_target="tpu_custom_call" | custom-call | flops 20000000000 | bytes 8388608 | tf_op jit(solution)/shard_map/attention/pallas_call | solution.py:337
  148.3 1.1 copy-done.1
  149.5 1.0 slice.26
  151.4 14.3 %all-to-all-start = ((bf16[8,50,512]{2,1,0:T(8,128)(2,1)}), bf16[8,50,512]{2,1,0:T(8,128)(2,1)S(1)}, u32[]{:S(2)}, u32[]{:S(2)}) async-start(bf16[8,50,512]{2,1,0:T(8,128)(2,1)} %all_to_all.8), calls=%async_computation.2 | async-start | bytes 917504 | tf_op jit(solution)/shard_map/all_to_all | solution.py:416
  166.0 13.7 %all-to-all-done = bf16[8,50,512]{2,1,0:T(8,128)(2,1)S(1)} async-done(((bf16[8,50,512]{2,1,0:T(8,128)(2,1)}), bf16[8,50,512]{2,1,0:T(8,128)(2,1)S(1)}, u32[]{:S(2)}, u32[]{:S(2)}) %all-to-all-start) | async-done | bytes 409632 | tf_op jit(solution)/shard_map/all_to_all | solution.py:416
  179.8 1.2 fusion.15
  181.0 1.0 fusion.17
  182.0 8.6 %reduce-scatter.3.cloned.1.call-done = bf16[384,512]{1,0:T(8,128)(2,1)} async-done(((bf16[384,2048]{1,0:T(8,128)(2,1)}), bf16[384,512]{1,0:T(8,128)(2,1)}) %reduce-scatter.3.cloned.1.call-update) | async-done | bytes 393232 | tf_op jit(solution)/shard_map/reduce_scatter | solution.py:362
  (43 shorter events, 4.6 us)
Async XLA Ops:
  7.2 80.3 %copy-start = (bf16[1,512,2048]{2,1,0:T(8,128)(2,1)S(1)}, bf16[1,512,2048]{2,1,0:T(8,128)(2,1)}, u32[]{:S(2)}) copy-start(bf16[1,512,2048]{2,1,0:T(8,128)(2,1)} %param.28) | copy-start | bytes 6291460
  7.2 3.6 %copy-start.9 = (s32[160,2]{0,1:T(2,128)S(1)}, s32[160,2]{0,1:T(2,128)}, u32[]{:S(2)}) copy-start(s32[160,2]{0,1:T(2,128)} %param.24) | copy-start | bytes 3844
  7.2 72.3 %all-gather.5.cloned.1.call-start = ((), (), s32[]{:S(2)}) async-start(), calls=%async_computation.5 | async-start | bytes 5406720 | tf_op jit(solution)/shard_map/all_gather | solution.py:396
  10.7 138.8 %reduce-scatter.5.cloned.1.call-start = ((), (), s32[]{:S(2)}) async-start(), calls=%async_computation.4 | async-start | bytes 2867200 | tf_op jit(solution)/shard_map/reduce_scatter | solution.py:414
  83.7 1.9 copy-start.11
  84.1 1.2 copy-start.8
  96.0 4.6 %copy-start.3 = (bf16[384,512]{1,0:T(8,128)(2,1)S(1)}, bf16[384,512]{1,0:T(8,128)(2,1)}, u32[]{:S(2)}) copy-start(bf16[384,512]{1,0:T(8,128)(2,1)} %v_ref.1) | copy-start | bytes 1179652
  96.0 4.6 %copy-start.6 = (f32[4]{0:T(128)S(1)}, f32[4]{0:T(128)}, u32[]{:S(2)}) copy-start(f32[4]{0:T(128)} %lam_ref.1) | copy-start | bytes 52
  96.0 4.6 %copy-start.7 = (f32[128]{0:T(128)S(1)}, f32[128]{0:T(128)}, u32[]{:S(2)}) copy-start(f32[128]{0:T(128)} %param.20) | copy-start | bytes 1540
  96.0 94.6 %reduce-scatter.3.cloned.1.call-start = ((), (), s32[]{:S(2)}) async-start(), calls=%async_computation.3 | async-start | bytes 1966080 | tf_op jit(solution)/shard_map/reduce_scatter | solution.py:362
  100.6 1.8 copy-start.2
  102.4 1.0 copy-start.4
  103.4 1.0 copy-start.5
  148.3 1.1 copy-start.1
  149.4 16.5 %copy-start.10 = (f32[160,2]{0,1:T(2,128)S(1)}, f32[160,2]{0,1:T(2,128)}, u32[]{:S(2)}) copy-start(f32[160,2]{0,1:T(2,128)} %param.25) | copy-start | bytes 3844
  151.4 28.2 %all-to-all-start = ((bf16[8,50,512]{2,1,0:T(8,128)(2,1)}), bf16[8,50,512]{2,1,0:T(8,128)(2,1)S(1)}, u32[]{:S(2)}, u32[]{:S(2)}) async-start(bf16[8,50,512]{2,1,0:T(8,128)(2,1)} %all_to_all.8), calls=%async_computation.2 | async-start | bytes 917504 | tf_op jit(solution)/shard_map/all_to_all | solution.py:416
Sparse Core Ops, SparseCore 0:
  11.4 68.0 all-gather.4
  96.1 35.3 reduce-scatter.4
  149.6 40.9 reduce-scatter.2

commit v2 on v1

--- a/solution.py
+++ b/solution.py
@@ -124,11 +124,13 @@
 
 
 def attention_kernel(
-    n, heads, lam_ref, gain_ref, rq_ref, rk_ref, v_ref, w_ref, out_ref,
+    n, heads, lam_ref, gain_ref, rq_ref, rk_ref, v_ref, w_ref, tok_ref, out_ref, arr_ref,
     q_buf, k_buf, v_buf, vt_buf, hn_send, hn_buf, w_buf, acc, m_buf, l_buf,
-    q_ss, q_rs, k_ss, k_rs, v_ss, v_rs, fk_ss, fk_rs, fv_ss, fv_rs, h_ss, h_rs, loc, w_sem,
+    q_ss, q_rs, k_ss, k_rs, v_ss, v_rs, fk_ss, fk_rs, fv_ss, fv_rs, h_ss, h_rs, loc, w_sem, t_ss, t_rs, x_ss, x_rs,
 ):
     me = lax.axis_index("ep")
+    my_tp = lax.axis_index("tp")
+    n_tp = arr_ref.shape[0]
     g = n // heads
     my_head, my_core = me // g, me % g
     rows = rk_ref.shape[1]
@@ -139,6 +141,8 @@
     barrier = pltpu.get_barrier_semaphore()
     for step in range(1, n):
         pl.semaphore_signal(barrier, inc=1, device_id={"ep": lax.rem(me + step, n)}, device_id_type=MESH)
+    for step in range(1, n_tp):
+        pl.semaphore_signal(barrier, inc=1, device_id={"tp": lax.rem(my_tp + step, n_tp)}, device_id_type=MESH)
     w_copy = pltpu.make_async_copy(w_ref, w_buf, w_sem)
     w_copy.start()
 
@@ -153,10 +157,11 @@
         pltpu.make_async_copy(q_src(me), q_buf.at[me], loc.at[0]),
         pltpu.make_async_copy(rk_ref.at[my_head], k_buf.at[me], loc.at[1]),
         pltpu.make_async_copy(v_src(me), v_buf.at[me], loc.at[2]),
+        pltpu.make_async_copy(tok_ref.at[me], arr_ref.at[my_tp, me], loc.at[3]),
     )
     for copy in own:
         copy.start()
-    pl.semaphore_wait(barrier, n - 1)
+    pl.semaphore_wait(barrier, n - 1 + n_tp - 1)
 
     def q_copy(dest):
         return pltpu.make_async_remote_copy(
@@ -173,6 +178,28 @@
             v_src(dest), v_buf.at[me], v_ss.at[dest], v_rs.at[me],
             device_id={"ep": dest}, device_id_type=MESH)
 
+    def tok_copy(dest):
+        return pltpu.make_async_remote_copy(
+            tok_ref.at[dest], arr_ref.at[my_tp, me], t_ss.at[dest], t_rs.at[me],
+            device_id={"ep": dest}, device_id_type=MESH)
+
+    def tok_arrival(source):
+        return pltpu.make_async_remote_copy(
+            tok_ref.at[0], arr_ref.at[my_tp, source], t_ss.at[0], t_rs.at[source],
+            device_id={"ep": lax.rem(me + 1, n)}, device_id_type=MESH)
+
+    def tok_spread(dest):
+        return pltpu.make_async_remote_copy(
+            arr_ref.at[my_tp], arr_ref.at[my_tp], x_ss.at[dest], x_rs.at[my_tp],
+            device_id={"tp": dest}, device_id_type=MESH)
+
+    def spread_arrival(source):
+        return pltpu.make_async_remote_copy(
+            arr_ref.at[source], arr_ref.at[source], x_ss.at[source], x_rs.at[source],
+            device_id={"tp": lax.rem(my_tp + 1, n_tp)}, device_id_type=MESH)
+
+    for step in range(1, n):
+        tok_copy(lax.rem(me + step, n)).start()
     for step in range(1, n):
         dest = lax.rem(me + step, n)
         if step % g == 0:
@@ -274,6 +301,14 @@
             return 0
 
         lax.fori_loop(0, g, member, 0)
+
+        @pl.when(p == 0)
+        def _():
+            for step in range(1, n):
+                tok_arrival(lax.rem(me + step, n)).wait_recv()
+            for step in range(1, n_tp):
+                tok_spread(lax.rem(my_tp + step, n_tp)).start()
+
         return 0
 
     def hn_copy(dest):
@@ -290,8 +325,10 @@
     for part in range(g):
         normed = jnp.concatenate(
             [hn_buf[h * g + lax.rem(part + me, g)] for h in range(heads)], axis=1)
-        out_ref[part * sub : (part + 1) * sub, :] = jnp.dot(
-            normed, w_buf[...], preferred_element_type=f32).astype(bf16)
+        for t in range(n_tp):
+            piece = out_ref.shape[2]
+            out_ref[t, part * sub : (part + 1) * sub, :] = jnp.dot(
+                normed, w_buf[:, t * piece : (t + 1) * piece], preferred_element_type=f32).astype(bf16)
     for step in range(1, n):
         dest = lax.rem(me + step, n)
         if step % g == 0:
@@ -299,6 +336,11 @@
             v_copy(dest).wait_send()
         q_copy(dest).wait_send()
         hn_copy(dest).wait_send()
+        tok_copy(dest).wait_send()
+    for step in range(1, n_tp):
+        other = lax.rem(my_tp + step, n_tp)
+        spread_arrival(other).wait_recv()
+        tok_spread(other).wait_send()
     for p in range(heads):
         for step in range(1, g):
             for copy in forward(p * g + my_core, step):
@@ -309,7 +351,7 @@
     return 2 * sub
 
 
-def exchange_attention(query_pairs, key_pairs, value_rows, head_lambda, head_gain, out_weight):
+def exchange_attention(query_pairs, key_pairs, value_rows, head_lambda, head_gain, out_weight, outgoing):
     n = lax.axis_size("ep")
     rows = query_pairs.shape[0]
     heads = head_lambda.shape[0]
@@ -334,11 +376,15 @@
     vmem = pl.BlockSpec(memory_space=pltpu.VMEM)
     dma = pltpu.SemaphoreType.DMA
     g = n // heads
-    terms = pl.pallas_call(
+    n_tp = lax.axis_size("tp")
+    return pl.pallas_call(
         functools.partial(attention_kernel, n, heads),
-        out_shape=jax.ShapeDtypeStruct((rows, out_weight.shape[1]), bf16),
-        in_specs=[pl.BlockSpec(memory_space=pltpu.SMEM), vmem, any_spec, any_spec, any_spec, any_spec],
-        out_specs=vmem,
+        out_shape=(
+            jax.ShapeDtypeStruct((n_tp, rows, out_weight.shape[1] // n_tp), bf16),
+            jax.ShapeDtypeStruct((n_tp,) + outgoing.shape, bf16),
+        ),
+        in_specs=[pl.BlockSpec(memory_space=pltpu.SMEM), vmem] + [any_spec] * 5,
+        out_specs=(vmem, any_spec),
         scratch_shapes=[
             pltpu.VMEM((n, sub, width), bf16),
             pltpu.VMEM((n, rows, width), bf16),
@@ -352,14 +398,182 @@
             pltpu.VMEM((1, 2 * sub), f32),
             dma((n,)), dma((n,)), dma((n,)), dma((n,)), dma((n,)), dma((n,)),
             dma((n, g)), dma((n,)), dma((n, g)), dma((n,)),
-            dma((n,)), dma((n,)), dma((3,)), dma(()),
+            dma((n,)), dma((n,)), dma((4,)), dma(()),
+            dma((n,)), dma((n,)), dma((n_tp,)), dma((n_tp,)),
         ],
         compiler_params=pltpu.CompilerParams(
             collective_id=0, has_side_effects=True, vmem_limit_bytes=40 * 2**20),
         cost_estimate=pl.CostEstimate(flops=20 * 10**9, bytes_accessed=8 * 2**20, transcendentals=5 * 10**6),
         name="attention",
-    )(head_lambda, head_gain.reshape(1, vw), rq, rk, value_rows, out_weight)
-    return lax.psum_scatter(terms, "tp", scatter_dimension=1, tiled=True)
+    )(head_lambda, head_gain.reshape(1, vw), rq, rk, value_rows, out_weight, outgoing)
+
+
+def expert_kernel(
+    n, n_tp, mix_ref, arr_ref, xn_ref, place_ref, rw_ref, wg_ref, wu_ref, wd_ref, sg_ref, su_ref, sd_ref,
+    attn_ref, moe_ref,
+    mix_in, arr, wg, wu, wd, sg, su, sd, sh_send, sh_in, ex_send, ex_in, y_buf, ret,
+    loc, m_ss, m_rs, s_ss, s_rs, e_ss, e_rs, y_ss, y_rs,
+):
+    me = lax.axis_index("ep")
+    my_tp = lax.axis_index("tp")
+    piece = moe_ref.shape[1]
+    cap = y_buf.shape[1]
+    barrier = pltpu.get_barrier_semaphore()
+    for step in range(1, n):
+        pl.semaphore_signal(barrier, inc=1, device_id={"ep": lax.rem(me + step, n)}, device_id_type=MESH)
+    for step in range(1, n_tp):
+        pl.semaphore_signal(barrier, inc=1, device_id={"tp": lax.rem(my_tp + step, n_tp)}, device_id_type=MESH)
+    loads = [
+        pltpu.make_async_copy(source, target, loc.at[i])
+        for i, (source, target) in enumerate((
+            (sg_ref, sg), (su_ref, su), (sd_ref, sd), (arr_ref, arr),
+            (wg_ref.at[0], wg), (wu_ref.at[0], wu), (wd_ref.at[0], wd),
+            (mix_ref.at[my_tp], mix_in.at[my_tp])))
+    ]
+    for load in loads:
+        load.start()
+    pl.semaphore_wait(barrier, n - 1 + n_tp - 1)
+
+    def scatter(send, into, send_sems, recv_sems, dest):
+        return pltpu.make_async_remote_copy(
+            send.at[dest], into.at[my_tp], send_sems.at[dest], recv_sems.at[my_tp],
+            device_id={"tp": dest}, device_id_type=MESH)
+
+    def arrival(into, recv_sems, source, axis):
+        return pltpu.make_async_remote_copy(
+            into.at[source], into.at[source], recv_sems.at[source], recv_sems.at[source],
+            device_id={axis: lax.rem(lax.axis_index(axis) + 1, n if axis == "ep" else n_tp)},
+            device_id_type=MESH)
+
+    peers = [lax.rem(my_tp + step, n_tp) for step in (*range(1, n_tp), 0)]
+    for dest in peers[:-1]:
+        scatter(mix_ref, mix_in, m_ss, m_rs, dest).start()
+
+    def columns(dest):
+        return pl.ds(pl.multiple_of(dest * piece, piece), piece)
+
+    def gated(gate, up):
+        return (gate / (1.0 + jnp.exp(-gate)) * up).astype(bf16)
+
+    for i in (0, 1, 2):
+        loads[i].wait()
+    xn = xn_ref[...]
+    hidden = gated(
+        jnp.dot(xn, sg[...], preferred_element_type=f32),
+        jnp.dot(xn, su[...], preferred_element_type=f32))
+    for dest in peers:
+        sh_send[dest] = jnp.dot(hidden, sd[:, columns(dest)], preferred_element_type=f32).astype(bf16)
+    for i in (3, 4, 5, 6):
+        loads[i].wait()
+    gate = up = None
+    for t in range(n_tp):
+        rows = arr[t].reshape(n * cap, piece)
+        span = slice(t * piece, (t + 1) * piece)
+        gate_part = jnp.dot(rows, wg[span, :], preferred_element_type=f32)
+        up_part = jnp.dot(rows, wu[span, :], preferred_element_type=f32)
+        gate = gate_part if gate is None else gate + gate_part
+        up = up_part if up is None else up + up_part
+    hidden = gated(gate, up)
+    for dest in peers:
+        ex_send[dest] = jnp.dot(hidden, wd[:, columns(dest)], preferred_element_type=f32).astype(bf16)
+        if dest is not peers[-1]:
+            scatter(ex_send, ex_in, e_ss, e_rs, dest).start()
+    for dest in peers[:-1]:
+        scatter(sh_send, sh_in, s_ss, s_rs, dest).start()
+    loads[7].wait()
+    for source in peers[:-1]:
+        arrival(mix_in, m_rs, source, "tp").wait_recv()
+    total = mix_in[0].astype(f32)
+    for t in range(1, n_tp):
+        total = total + mix_in[t].astype(f32)
+    attn_ref[...] = total.astype(bf16)
+
+    def y_copy(dest):
+        return pltpu.make_async_remote_copy(
+            y_buf.at[dest], ret.at[me], y_ss.at[dest], y_rs.at[me],
+            device_id={"ep": dest}, device_id_type=MESH)
+
+    y = ex_send[my_tp].astype(f32)
+    for source in peers[:-1]:
+        arrival(ex_in, e_rs, source, "tp").wait_recv()
+        y = y + ex_in[source].astype(f32)
+    y_buf[...] = y.astype(bf16).reshape(n, cap, piece)
+    for step in range(1, n):
+        y_copy(lax.rem(me + step, n)).start()
+    ret[me] = y_buf[me]
+    out = sh_send[my_tp].astype(f32)
+    for source in peers[:-1]:
+        arrival(sh_in, s_rs, source, "tp").wait_recv()
+        out = out + sh_in[source].astype(f32)
+    for step in range(1, n):
+        arrival(ret, y_rs, lax.rem(me + step, n), "ep").wait_recv()
+    returned = ret[...].reshape(n * cap, piece)
+    for k in range(place_ref.shape[0]):
+        out = out + rw_ref[:, k : k + 1] * jnp.dot(place_ref[k], returned, preferred_element_type=f32)
+    moe_ref[...] = out.astype(bf16)
+    for dest in peers[:-1]:
+        scatter(mix_ref, mix_in, m_ss, m_rs, dest).wait_send()
+        scatter(ex_send, ex_in, e_ss, e_rs, dest).wait_send()
+        scatter(sh_send, sh_in, s_ss, s_rs, dest).wait_send()
+    for step in range(1, n):
+        y_copy(lax.rem(me + step, n)).wait_send()
+
+
+def exchange_all(
+    query_pairs, key_pairs, value_rows, head_lambda, head_gain, out_weight, normed, routes, route_weight,
+    gate_weight, up_weight, down_weight, shared_gate, shared_up, shared_down,
+):
+    n, n_tp = lax.axis_size("ep"), lax.axis_size("tp")
+    tokens, model = normed.shape
+    piece = model // n_tp
+    rows = query_pairs.shape[0]
+    cap = -(-(tokens * TOP_K * 5 // (4 * n)) // 16) * 16
+    onehot = (routes[:, :, None] == jnp.arange(n, dtype=jnp.int32)).astype(bf16)
+    lower = jnp.tril(jnp.ones((tokens, tokens), bf16))
+    ranks = jnp.dot(lower, jnp.sum(onehot, axis=1), preferred_element_type=f32) - 1.0
+    slots = jnp.sum(onehot.astype(f32) * (ranks[:, None, :] + jnp.arange(n, dtype=f32) * cap), axis=-1)
+    slots = slots.astype(jnp.int32).T
+    place = (slots[:, :, None] == jnp.arange(n * cap, dtype=jnp.int32)).astype(bf16)
+    part = lax.dynamic_slice_in_dim(normed, lax.axis_index("tp") * piece, piece, axis=1)
+    outgoing = lax.dot_general(
+        jnp.sum(place, axis=0), part, (((0,), (0,)), ((), ())), preferred_element_type=f32).astype(bf16)
+    mix, arr = exchange_attention(
+        query_pairs, key_pairs, value_rows, head_lambda, head_gain, out_weight, outgoing.reshape(n, cap, piece))
+    any_spec = pl.BlockSpec(memory_space=pl.ANY)
+    vmem = pl.BlockSpec(memory_space=pltpu.VMEM)
+    dma = pltpu.SemaphoreType.DMA
+    hidden, shared = gate_weight.shape[2], shared_gate.shape[1]
+    return pl.pallas_call(
+        functools.partial(expert_kernel, n, n_tp),
+        out_shape=(
+            jax.ShapeDtypeStruct((rows, piece), bf16),
+            jax.ShapeDtypeStruct((tokens, piece), bf16),
+        ),
+        in_specs=[any_spec, any_spec, vmem, vmem, vmem] + [any_spec] * 6,
+        out_specs=(vmem, vmem),
+        scratch_shapes=[
+            pltpu.VMEM((n_tp, rows, piece), bf16),
+            pltpu.VMEM((n_tp, n, cap, piece), bf16),
+            pltpu.VMEM((model, hidden), bf16),
+            pltpu.VMEM((model, hidden), bf16),
+            pltpu.VMEM((hidden, model), bf16),
+            pltpu.VMEM((model, shared), bf16),
+            pltpu.VMEM((model, shared), bf16),
+            pltpu.VMEM((shared, model), bf16),
+            pltpu.VMEM((n_tp, tokens, piece), bf16),
+            pltpu.VMEM((n_tp, tokens, piece), bf16),
+            pltpu.VMEM((n_tp, n * cap, piece), bf16),
+            pltpu.VMEM((n_tp, n * cap, piece), bf16),
+            pltpu.VMEM((n, cap, piece), bf16),
+            pltpu.VMEM((n, cap, piece), bf16),
+            dma((8,)), dma((n_tp,)), dma((n_tp,)), dma((n_tp,)), dma((n_tp,)), dma((n_tp,)), dma((n_tp,)),
+            dma((n,)), dma((n,)),
+        ],
+        compiler_params=pltpu.CompilerParams(
+            collective_id=1, has_side_effects=True, vmem_limit_bytes=48 * 2**20),
+        cost_estimate=pl.CostEstimate(flops=10 * 10**9, bytes_accessed=16 * 2**20, transcendentals=5 * 10**5),
+        name="experts",
+    )(mix, arr, normed, place, route_weight, gate_weight, up_weight, down_weight, shared_gate, shared_up, shared_down)
 
 
 def local(
@@ -384,24 +598,29 @@
     heads = head_lambda.shape[0]
     rows = query_pairs.shape[0]
     fits = n % heads == 0 and n // heads > 1 and (rows * heads) % (n * 64) == 0
-    attention = exchange_attention if fits else generic_attention
-    attn_out = attention(query_pairs, key_pairs, value_rows, head_lambda, head_gain, out_weight)
     row_values = moe_input.astype(jnp.float32)
     inverse_norm = lax.rsqrt(jnp.mean(row_values * row_values, axis=-1, keepdims=True) + norm_eps)
     normed = (row_values * inverse_norm * ffn_gain).astype(jnp.bfloat16)
-    tokens, model = normed.shape
-    n_tp = lax.axis_size("tp")
-    capacity = tokens * TOP_K * 5 // (4 * n)
-    part = lax.dynamic_slice_in_dim(normed, lax.axis_index("tp") * (model // n_tp), model // n_tp, axis=1)
-    gathered = lax.all_gather(part, ("ep", "tp"), axis=0, tiled=False)
-    gathered = gathered.reshape(n, n_tp, tokens, model // n_tp)
-    all_routes = lax.all_gather(routes, "ep", axis=0, tiled=False)
-    hit = jnp.any(all_routes == lax.axis_index("ep"), axis=-1)
-    lower = jnp.tril(jnp.ones((tokens, tokens), bf16))
-    rank = jnp.dot(hit.astype(bf16), lower.T, preferred_element_type=f32).astype(jnp.int32) - 1
-    select = (hit[:, None, :] & (rank[:, None, :] == jnp.arange(capacity, dtype=jnp.int32)[None, :, None])).astype(bf16)
-    arrived = jnp.einsum("bst,bhtd->bshd", select, gathered, preferred_element_type=f32).astype(bf16)
-    arrived = arrived.reshape(n * capacity, model)
+    if fits:
+        return exchange_all(
+            query_pairs, key_pairs, value_rows, head_lambda, head_gain, out_weight, normed, routes, route_weight,
+            gate_weight, up_weight, down_weight, shared_gate, shared_up, shared_down,
+        )
+    attn_out = generic_attention(query_pairs, key_pairs, value_rows, head_lambda, head_gain, out_weight)
+    token_rows = normed.shape[0]
+    experts = lax.axis_size("ep")
+    capacity = token_rows * TOP_K * 5 // (4 * experts)
+    flat_routes = routes.reshape(-1)
+    onehot = (flat_routes[:, None] == jnp.arange(experts, dtype=jnp.int32)).astype(jnp.int32)
+    slot_rank = jnp.sum((jnp.cumsum(onehot, axis=0) - 1) * onehot, axis=-1)
+    slot_index = flat_routes * capacity + slot_rank
+    token_index = jnp.arange(token_rows * TOP_K, dtype=jnp.int32) // TOP_K
+    slot_rows = (
+        jnp.full((experts * capacity,), token_rows, jnp.int32).at[slot_index].set(token_index)
+    )
+    padded = jnp.concatenate([normed, jnp.zeros((1, normed.shape[1]), jnp.bfloat16)], axis=0)
+    outgoing = padded[slot_rows]
+    arrived = lax.all_to_all(outgoing, "ep", split_axis=0, concat_axis=0, tiled=True)
     gate_part = jnp.dot(arrived, gate_weight[0], preferred_element_type=jnp.float32)
     up_part = jnp.dot(arrived, up_weight[0], preferred_element_type=jnp.float32)
     hidden = (jax.nn.silu(gate_part) * up_part).astype(jnp.bfloat16)
@@ -410,20 +629,21 @@
     shared_lifted = jnp.dot(normed, shared_up, preferred_element_type=jnp.float32)
     shared_hidden = (jax.nn.silu(shared_gated) * shared_lifted).astype(jnp.bfloat16)
     shared_terms = jnp.dot(shared_hidden, shared_down, preferred_element_type=jnp.float32)
-    both = jnp.concatenate([expert_terms.astype(bf16), shared_terms.astype(bf16)], axis=0)
-    sums = lax.psum_scatter(both, "tp", scatter_dimension=1, tiled=True)
-    expert_sum, shared_sum = sums[: n * capacity], sums[n * capacity :].astype(f32)
-    returned = lax.all_to_all(expert_sum, "ep", split_axis=0, concat_axis=0, tiled=True)
-    onehot = (routes[:, :, None] == jnp.arange(n, dtype=jnp.int32)).astype(bf16)
-    named = jnp.sum(onehot, axis=1)
-    ranks = jnp.dot(lower, named, preferred_element_type=f32) - 1.0
-    slots = jnp.sum(onehot.astype(f32) * (ranks[:, None, :] + jnp.arange(n, dtype=f32) * capacity), axis=-1)
-    moe_out = shared_sum
-    for k in range(TOP_K):
-        place = (slots[:, k : k + 1].astype(jnp.int32) == jnp.arange(n * capacity, dtype=jnp.int32)).astype(bf16)
-        picked = jnp.dot(place, returned, preferred_element_type=f32)
-        moe_out = moe_out + route_weight[:, k : k + 1] * picked
-    moe_out = moe_out.astype(bf16)
+    expert_sum, shared_sum = (
+        lax.psum_scatter(
+            expert_terms.astype(jnp.bfloat16), "tp", scatter_dimension=1, tiled=True
+        ).astype(jnp.float32),
+        lax.psum_scatter(
+            shared_terms.astype(jnp.bfloat16), "tp", scatter_dimension=1, tiled=True
+        ).astype(jnp.float32),
+    )
+    returned = lax.all_to_all(
+        expert_sum.astype(jnp.bfloat16), "ep", split_axis=0, concat_axis=0, tiled=True
+    )
+    picked = returned[slot_index.reshape(token_rows, TOP_K)]
+    moe_out = (
+        jnp.sum(route_weight[..., None] * picked.astype(jnp.float32), axis=1) + shared_sum
+    ).astype(jnp.bfloat16)
     return (attn_out, moe_out)
 
 

time: 198 us -> 143 us (0.72)
  Pallas kernels: 46.5 us -> 128 us
  waiting for transfers between devices: 70.2 us -> 0 us
  matrix products: 19.2 us -> 0.46 us
  blocking collectives: 14.5 us -> 0 us
  starting transfers between devices: 14.4 us -> 0 us
  between operations: 13.9 us -> 0.82 us
  local copies, waits for them, and re-layouts: 10.4 us -> 7.06 us
  other arithmetic: 7.86 us -> 5.15 us
    pallas_call x1 -> x2, Pallas kernels: 43.9 us -> 126 us  [the longest x1 67 us: exchange_all(): pl.pallas_call(functools.partial(expert_kernel, n, n_tp), out_shape=(jax....]
    all_gather x1 -> x0, waiting for transfers between devices: 47.9 us -> none  [local(): gathered = lax.all_gather(part, ('ep', 'tp'), axis=0, tiled=False)]
    dot_general x9 -> x2, matrix products: 19.2 us -> 0.46 us  [the longest x1 0.34 us: exchange_all(): lax.dot_general(jnp.sum(place, axis=0), part, (((0,), (0,)), ((), ())), p...]
    all_gather x1 -> x0, blocking collectives: 14.5 us -> none  [local(): all_routes = lax.all_gather(routes, 'ep', axis=0, tiled=False)]
    all_to_all x1 -> x0, starting transfers between devices: 14.3 us -> none  [local(): lax.all_to_all(expert_sum, 'ep', split_axis=0, concat_axis=0, tiled=True)]
    all_to_all x1 -> x0, waiting for transfers between devices: 13.7 us -> none  [local(): lax.all_to_all(expert_sum, 'ep', split_axis=0, concat_axis=0, tiled=True)]
    reduce_scatter x2 -> x0, waiting for transfers between devices: 8.59 us -> none  [the longest x1 8.57 us: exchange_attention(): return lax.psum_scatter(terms, 'tp', scatter_dimension=1, tiled=True)]
    concatenate x1 -> x0, other arithmetic: 3.05 us -> none  [local(): jnp.concatenate([expert_terms.astype(bf16), shared_terms.astype(bf16)], a...]
  transfers between devices with their start and end apart: 4 -> 0, of which waited for: 3 -> 0; matrix products, arithmetic and copies ran while one was open for 6% -> 0% of each run, Pallas kernels for 24% -> 0%
where the time goes in v2:
time: 143 us; the launch traced here: 142 us
  Pallas kernels  128 us (90%)
  local copies, waits for them, and re-layouts  7.06 us (5%)
  other arithmetic  5.15 us (4%)
    pallas_call x1, Pallas kernels, exchange_all(): pl.pallas_call(functools.partial(expert_kernel, n, n_tp), out_shape=(jax....  67 us
    pallas_call x1, Pallas kernels, exchange_attention(): pl.pallas_call(functools.partial(attention_kernel, n, heads), out_shape=(...  58.7 us
    unnamed x29, local copies, waits for them, and re-layouts  7.06 us

profile of v2, /device:TPU:0, one launch (start us, length us, event | category | flops | bytes accessed | tf_op | source)
XLA Modules:
  0.0 141.9 jit_solution(12662268171563008490)
XLA Ops:
  0.6 0.0 copy-start.10
  0.7 0.8 fusion.9
  1.5 1.1 pad_maximum_fusion
  2.6 2.8 %rotate.1 = (bf16[4,384,128]{2,1,0:T(8,128)(2,1)}, bf16[4,384,128]{2,1,0:T(8,128)(2,1)}) custom-call(bf16[384,512]{1,0:T(8,128)(2,1)} %q_ref.1, bf16[384,512]{1,0:T(8,128)(2,1)} %k_ref.1, f32[384,128]{1,0:T(8,128)} %get-tuple-element.13.cos_ref, f32[384,128]{1,0:T(8,128)} %get-tuple-element.14.sin_ref), custom_call_target="tpu_custom_call" | custom-call | tf_op jit(solution)/shard_map/rotate/pallas_call | solution.py:370
  5.4 0.2 fusion
  5.6 1.3 fusion.2.xn_ref
  6.9 0.7 fusion.13
  7.6 0.1 fusion.3
  7.7 0.8 multiply_reduce_fusion
  8.5 0.1 fusion.7
  8.6 0.3 convolution_convert_fusion
  9.0 0.0 copy-done
  9.0 0.0 copy-done.1
  9.0 0.0 copy-start.12
  9.1 58.7 %attention.1 = (bf16[4,384,512]{2,1,0:T(8,128)(2,1)S(1)}, bf16[4,8,64,512]{3,2,1,0:T(8,128)(2,1)S(1)}) custom-call(f32[4]{0:T(128)S(1)} %copy-done.4, f32[1,128]{1,0:T(1,128)S(1)} %bitcast.7, bf16[4,384,128]{2,1,0:T(8,128)(2,1)S(1)} %copy-done.2, bf16[4,384,128]{2,1,0:T(8,128)(2,1)S(1)} %copy-done.3, bf16[384,512]{1,0:T(8,128)(2,1)S(1)} %copy-done.1, ...), custom_call_target="tpu_custom_call" | custom-call | flops 20000000000 | bytes 8388608 | tf_op jit(solution)/shard_map/attention/pallas_call | solution.py:380
  67.8 1.3 copy-done.6
  69.1 1.1 copy-done.8
  70.3 0.1 fusion.4.place_ref
  70.4 0.1 copy.23.rw_ref
  70.5 1.6 %copy-done.7 = bf16[4,8,64,512]{3,2,1,0:T(8,128)(2,1)S(1)} copy-done((bf16[4,8,64,512]{3,2,1,0:T(8,128)(2,1)S(1)}, bf16[4,8,64,512]{3,2,1,0:T(8,128)(2,1)}, u32[]{:S(2)}) %copy-start.7) | copy-done | bytes 2097176
  72.1 1.4 copy-done.9
  73.5 67.0 %experts.1 = (bf16[384,512]{1,0:T(8,128)(2,1)S(1)}, bf16[160,512]{1,0:T(8,128)(2,1)S(1)}) custom-call(bf16[4,384,512]{2,1,0:T(8,128)(2,1)S(1)} %copy-done.9, bf16[4,8,64,512]{3,2,1,0:T(8,128)(2,1)S(1)} %copy-done.7, bf16[160,2048]{1,0:T(8,128)(2,1)S(1)} %fusion.2.xn_ref, bf16[2,160,512]{2,1,0:T(8,128)(2,1)S(1)} %fusion.4.place_ref, ...), custom_call_target="tpu_custom_call" | custom-call | flops 10000000000 | bytes 16777216 | tf_op jit(solution)/shard_map/experts/pallas_call | solution.py:546
  140.5 0.7 copy.26
  141.2 0.7 copy.27
  (23 shorter events, 0.1 us)
Async XLA Ops:
  0.6 4.7 %copy-start.10 = (bf16[160,2048]{1,0:T(8,128)(2,1)S(1)}, bf16[160,2048]{1,0:T(8,128)(2,1)}, u32[]{:S(2)}) copy-start(bf16[160,2048]{1,0:T(8,128)(2,1)} %param.22) | copy-start | bytes 1966084
  0.6 5.0 %copy-start.11 = (f32[2048]{0:T(1024)S(1)}, f32[2048]{0:T(1024)}, u32[]{:S(2)}) copy-start(f32[2048]{0:T(1024)} %param.23) | copy-start | bytes 24580
  2.6 6.4 %copy-start = (bf16[512,2048]{1,0:T(8,128)(2,1)S(1)}, bf16[512,2048]{1,0:T(8,128)(2,1)}, u32[]{:S(2)}) copy-start(bf16[512,2048]{1,0:T(8,128)(2,1)} %w_ref.1) | copy-start | bytes 6291460
  2.6 6.4 %copy-start.1 = (bf16[384,512]{1,0:T(8,128)(2,1)S(1)}, bf16[384,512]{1,0:T(8,128)(2,1)}, u32[]{:S(2)}) copy-start(bf16[384,512]{1,0:T(8,128)(2,1)} %v_ref.1) | copy-start | bytes 1179652
  2.6 6.4 %copy-start.4 = (f32[4]{0:T(128)S(1)}, f32[4]{0:T(128)}, u32[]{:S(2)}) copy-start(f32[4]{0:T(128)} %lam_ref.1) | copy-start | bytes 52
  2.6 6.4 %copy-start.5 = (f32[128]{0:T(128)S(1)}, f32[128]{0:T(128)}, u32[]{:S(2)}) copy-start(f32[128]{0:T(128)} %param.20) | copy-start | bytes 1540
  5.4 3.7 %copy-start.2 = (bf16[4,384,128]{2,1,0:T(8,128)(2,1)S(1)}, bf16[4,384,128]{2,1,0:T(8,128)(2,1)}, u32[]{:S(2)}) copy-start(bf16[4,384,128]{2,1,0:T(8,128)(2,1)} %get-tuple-element.6.rq_ref) | copy-start | bytes 1179652
  5.4 3.7 %copy-start.3 = (bf16[4,384,128]{2,1,0:T(8,128)(2,1)S(1)}, bf16[4,384,128]{2,1,0:T(8,128)(2,1)}, u32[]{:S(2)}) copy-start(bf16[4,384,128]{2,1,0:T(8,128)(2,1)} %get-tuple-element.7.rk_ref) | copy-start | bytes 1179652
  9.0 61.3 %copy-start.12 = (f32[160,2]{0,1:T(2,128)S(1)}, f32[160,2]{0,1:T(2,128)}, u32[]{:S(2)}) copy-start(f32[160,2]{0,1:T(2,128)} %param.25) | copy-start | bytes 3844
  67.7 1.4 copy-start.6
  69.1 1.2 copy-start.8
  70.5 1.6 %copy-start.7 = (bf16[4,8,64,512]{3,2,1,0:T(8,128)(2,1)S(1)}, bf16[4,8,64,512]{3,2,1,0:T(8,128)(2,1)}, u32[]{:S(2)}) copy-start(bf16[4,8,64,512]{3,2,1,0:T(8,128)(2,1)} %copy-done.6) | copy-start | bytes 6291460
  72.1 1.4 copy-start.9

commit v3 on v2

--- a/solution.py
+++ b/solution.py
@@ -402,7 +402,7 @@
             dma((n,)), dma((n,)), dma((n_tp,)), dma((n_tp,)),
         ],
         compiler_params=pltpu.CompilerParams(
-            collective_id=0, has_side_effects=True, vmem_limit_bytes=40 * 2**20),
+            collective_id=0, has_side_effects=True, vmem_limit_bytes=56 * 2**20),
         cost_estimate=pl.CostEstimate(flops=20 * 10**9, bytes_accessed=8 * 2**20, transcendentals=5 * 10**6),
         name="attention",
     )(head_lambda, head_gain.reshape(1, vw), rq, rk, value_rows, out_weight, outgoing)
@@ -527,7 +527,7 @@
     tokens, model = normed.shape
     piece = model // n_tp
     rows = query_pairs.shape[0]
-    cap = -(-(tokens * TOP_K * 5 // (4 * n)) // 16) * 16
+    cap = -(-(tokens * TOP_K * 5 // (4 * n)) // 8) * 8
     onehot = (routes[:, :, None] == jnp.arange(n, dtype=jnp.int32)).astype(bf16)
     lower = jnp.tril(jnp.ones((tokens, tokens), bf16))
     ranks = jnp.dot(lower, jnp.sum(onehot, axis=1), preferred_element_type=f32) - 1.0
@@ -570,7 +570,7 @@
             dma((n,)), dma((n,)),
         ],
         compiler_params=pltpu.CompilerParams(
-            collective_id=1, has_side_effects=True, vmem_limit_bytes=48 * 2**20),
+            collective_id=1, has_side_effects=True, vmem_limit_bytes=60 * 2**20),
         cost_estimate=pl.CostEstimate(flops=10 * 10**9, bytes_accessed=16 * 2**20, transcendentals=5 * 10**5),
         name="experts",
     )(mix, arr, normed, place, route_weight, gate_weight, up_weight, down_weight, shared_gate, shared_up, shared_down)

time: 143 us -> 137 us (0.958)
  local copies, waits for them, and re-layouts: 7.06 us -> 4.14 us
  other arithmetic: 5.15 us -> 3.4 us
    unnamed x29 -> x13, local copies, waits for them, and re-layouts: 7.06 us -> 4.14 us
    pallas_call x1, Pallas kernels: 67 us -> 65.5 us  [exchange_all(): pl.pallas_call(functools.partial(expert_kernel, n, n_tp), out_shape=(jax....]
where the time goes in v3:
time: 137 us; the launch traced here: 136 us
  Pallas kernels  127 us (93%)
  local copies, waits for them, and re-layouts  4.14 us (3%)
  other arithmetic  3.4 us (2%)
    pallas_call x1, Pallas kernels, exchange_all(): pl.pallas_call(functools.partial(expert_kernel, n, n_tp), out_shape=(jax....  65.5 us
    pallas_call x1, Pallas kernels, exchange_attention(): pl.pallas_call(functools.partial(attention_kernel, n, heads), out_shape=(...  58.9 us
    unnamed x13, local copies, waits for them, and re-layouts  4.14 us

profile of v3, /device:TPU:0, one launch (start us, length us, event | category | flops | bytes accessed | tf_op | source)
XLA Modules:
  0.0 136.5 jit_solution(16845973564310978378)
XLA Ops:
  0.6 0.0 copy-start
  0.6 0.0 copy-start.2
  0.7 0.8 fusion.9
  1.5 0.0 copy-start.3
  1.5 1.1 pad_maximum_fusion
  2.6 2.6 %rotate.1 = (bf16[4,384,128]{2,1,0:T(8,128)(2,1)}, bf16[4,384,128]{2,1,0:T(8,128)(2,1)}) custom-call(bf16[384,512]{1,0:T(8,128)(2,1)} %q_ref.1, bf16[384,512]{1,0:T(8,128)(2,1)} %k_ref.1, f32[384,128]{1,0:T(8,128)} %get-tuple-element.13.cos_ref, f32[384,128]{1,0:T(8,128)} %get-tuple-element.14.sin_ref), custom_call_target="tpu_custom_call" | custom-call | tf_op jit(solution)/shard_map/rotate/pallas_call | solution.py:370
  5.2 0.0 copy-done
  5.2 0.2 fusion
  5.4 0.0 copy-done.2
  5.4 0.2 fusion.2.xn_ref
  5.6 0.0 copy-done.3
  5.7 0.0 copy-start.1
  5.7 0.1 fusion.3
  5.8 0.1 multiply_reduce_fusion
  5.9 0.1 fusion.7
  6.0 1.1 convolution_convert_fusion
  7.1 58.9 %attention.1 = (bf16[4,384,512]{2,1,0:T(8,128)(2,1)}, bf16[4,8,56,512]{3,2,1,0:T(8,128)(2,1)}) custom-call(f32[4]{0:T(128)} %lam_ref.1, f32[1,128]{1,0:T(1,128)} %bitcast.7, bf16[4,384,128]{2,1,0:T(8,128)(2,1)} %get-tuple-element.6.rq_ref, bf16[4,384,128]{2,1,0:T(8,128)(2,1)} %get-tuple-element.7.rk_ref, bf16[384,512]{1,0:T(8,128)(2,1)} %v_ref.1, ...), custom_call_target="tpu_custom_call" | custom-call | flops 20000000000 | bytes 8388608 | tf_op jit(solution)/shard_map/attention/pallas_call | solution.py:380
  66.0 0.0 copy-done.1
  66.0 0.8 fusion.4.place_ref
  66.8 0.0 copy-done.4
  66.9 0.8 copy.23.rw_ref
  67.6 65.5 %experts.1 = (bf16[384,512]{1,0:T(8,128)(2,1)}, bf16[160,512]{1,0:T(8,128)(2,1)}) custom-call(bf16[4,384,512]{2,1,0:T(8,128)(2,1)} %get-tuple-element.8.mix_ref, bf16[4,8,56,512]{3,2,1,0:T(8,128)(2,1)} %get-tuple-element.9.arr_ref, bf16[160,2048]{1,0:T(8,128)(2,1)} %copy-done.1, bf16[2,160,448]{2,1,0:T(8,128)(2,1)} %fusion.4.place_ref, ...), custom_call_target="tpu_custom_call" | custom-call | flops 10000000000 | bytes 16777216 | tf_op jit(solution)/shard_map/experts/pallas_call | solution.py:546
  133.1 1.8 %copy.26 = bf16[384,512]{1,0:T(8,128)(2,1)} copy(bf16[384,512]{1,0:T(8,128)(2,1)} %get-tuple-element.17) | data formatting | bytes 786432
  134.9 1.6 %copy.27 = bf16[160,512]{1,0:T(8,128)(2,1)} copy(bf16[160,512]{1,0:T(8,128)(2,1)} %get-tuple-element.18) | data formatting | bytes 327680
  (7 shorter events, 0.0 us)
Async XLA Ops:
  0.6 4.6 %copy-start = (bf16[160,2048]{1,0:T(8,128)(2,1)S(1)}, bf16[160,2048]{1,0:T(8,128)(2,1)}, u32[]{:S(2)}) copy-start(bf16[160,2048]{1,0:T(8,128)(2,1)} %param.22) | copy-start | bytes 1966084
  0.6 4.8 %copy-start.2 = (f32[2048]{0:T(1024)S(1)}, f32[2048]{0:T(1024)}, u32[]{:S(2)}) copy-start(f32[2048]{0:T(1024)} %param.23) | copy-start | bytes 24580
  1.5 4.2 %copy-start.3 = (s32[160,2]{0,1:T(2,128)S(1)}, s32[160,2]{0,1:T(2,128)}, u32[]{:S(2)}) copy-start(s32[160,2]{0,1:T(2,128)} %param.24) | copy-start | bytes 3844
  5.7 60.3 %copy-start.1 = (bf16[160,2048]{1,0:T(8,128)(2,1)}, bf16[160,2048]{1,0:T(8,128)(2,1)S(1)}, u32[]{:S(2)}) copy-start(bf16[160,2048]{1,0:T(8,128)(2,1)S(1)} %fusion.2.xn_ref) | copy-start | bytes 1966084
  7.1 59.7 %copy-start.4 = (f32[160,2]{0,1:T(2,128)S(1)}, f32[160,2]{0,1:T(2,128)}, u32[]{:S(2)}) copy-start(f32[160,2]{0,1:T(2,128)} %param.25) | copy-start | bytes 3844
